TPU v7x, 256 devices: a whole 4x4x8 slice. The times are simulated.
256 devices in a mesh: ep: 64 (over z, y, core), tp: 4 (over x).
Axes of the slice: x: 4, y: 4, z: 8, core: 2. Of those that a mesh axis runs over, the one named last changes fastest.
Arguments:
- tokens: bfloat16 [1024, 2048], P('ep'), may hold values from -6 to 6
- norm_gain: float32 [2048], replicated, may hold values from 0.1 to 1.9
- query_weight: bfloat16 [2048, 1024], P(None, 'tp'), may hold values from -0.21875 to 0.21875
- key_weight: bfloat16 [2048, 512], P(None, 'tp'), may hold values from -0.125 to 0.125
- value_weight: bfloat16 [2048, 512], P(None, 'tp'), may hold values from -0.125 to 0.125
- output_weight: bfloat16 [1024, 2048], P('tp'), may hold values from -0.1875 to 0.1875
- head_gain: float32 [128], replicated, may hold values from 0.1 to 1.9
- lambdas: float32 [8], P('tp'), may hold values from 0.3 to 0.8
- key_cache: bfloat16 [1024, 1024, 4, 128], P('ep', None, 'tp')
- value_cache: bfloat16 [1024, 1024, 4, 128], P('ep', None, 'tp'), may hold values from -6 to 6
- lengths: int32 [1024], P('ep'), may hold values from 128 to 1024, as said below
- ffn_gain: float32 [2048], replicated, may hold values from 0.1 to 1.9
- routes: int32 [1024, 4], P('ep'), may hold values from 0 to 63, all different within a row; in each aligned block of 16 rows (0 to 15, 16 to 31, ...) at most 2 rows name the same one
- route_weight: float32 [1024, 4], P('ep'), may hold values from 0.1 to 1
- expert_gate: bfloat16 [64, 2048, 1024], P('ep', None, 'tp'), may hold values from -0.125 to 0.125
- expert_up: bfloat16 [64, 2048, 1024], P('ep', None, 'tp'), may hold values from -0.125 to 0.125
- expert_down: bfloat16 [64, 1024, 2048], P('ep', 'tp'), may hold values from -0.1875 to 0.1875
- dense_gate: bfloat16 [2048, 2048], P('tp'), may hold values from -0.125 to 0.125
- dense_up: bfloat16 [2048, 2048], P('tp'), may hold values from -0.125 to 0.125
- dense_down: bfloat16 [2048, 2048], P('tp'), may hold values from -0.1875 to 0.1875
- gate_vector: float32 [2048], P('tp')
Outputs:
- layer_out: bfloat16 [1024, 2048], P('ep', 'tp')
Inputs may be any that keep to these rules, and one draw needn't show every extreme that they name: `routes`: each row names 4 different experts. Among the rows of one index of ep no expert is named by more than 2 rows, a bound that some block reaches. `lengths`: some sequence has length 1024. Cached positions at or past a sequence's length are not read.
All inputs are finite; a program needn't handle non-finite values.
Results may differ from a plain program's by a relative error of at most 0.015.
The roundings to bfloat16 on the way count: a program that leaves them out, or rounds other values in their place, can miss the bound.
Values may be sent and summed in bfloat16 or wider, within the bound.
No kernel may reach another device: no remote copies, remote signals or barrier semaphores. Data moves between devices by JAX's collectives and lax.ppermute only.
A program may use at most 128 MiB of HBM per device.

v0:
```python
import jax
import jax.numpy as jnp
from jax import lax
from jax.sharding import PartitionSpec as P

HEADS = 8
KV_HEADS = 4
DQK = 64
DV = 128
TOPK = 4


epsilon = 1e-06


def from_everyone(shard, axis):
    devices = lax.axis_size(axis)
    return lax.all_to_all(
        jnp.broadcast_to(shard[None], (devices, *shard.shape)), axis, 0, 0, tiled=True
    )


def taken_together(shard, axis):
    return from_everyone(shard, axis).astype(jnp.float32).sum(axis=0)


def of_everyone(shard, axis):
    everything = from_everyone(shard, axis)
    return jnp.sum(everything, axis=0)


def cut_along(shard, dim, devices):
    before, after = (shard.shape[:dim], shard.shape[dim + 1 :])
    return jnp.moveaxis(shard.reshape(*before, devices, -1, *after), dim, 0)


def sent_and_summed(shard, axis, dim):
    devices = lax.axis_size(axis)
    blocks = lax.all_to_all(cut_along(shard, dim, devices), axis, 0, 0, tiled=True)
    return jnp.sum(blocks.astype(jnp.float32), axis=0)


def rms_scale(values, gain):
    return values * lax.rsqrt(jnp.mean(values * values, axis=-1, keepdims=True) + epsilon) * gain


def expert_hidden_rows(flat_rows, expert_gate, expert_up):
    expert_pre = jnp.dot(flat_rows, expert_gate[0], preferred_element_type=jnp.float32)
    expert_upper = jnp.dot(flat_rows, expert_up[0], preferred_element_type=jnp.float32)
    return (jax.nn.silu(expert_pre) * expert_upper).astype(jnp.bfloat16)


def shards(
    tokens,
    norm_gain,
    query_weight,
    key_weight,
    value_weight,
    output_weight,
    head_gain,
    lambdas,
    key_cache,
    value_cache,
    lengths,
    ffn_gain,
    routes,
    route_weight,
    expert_gate,
    expert_up,
    expert_down,
    dense_gate,
    dense_up,
    dense_down,
    gate_vector,
):
    seq_count = tokens.shape[0]
    model_width = tokens.shape[1]
    cache_len = key_cache.shape[1]
    local_kv = key_cache.shape[2]
    group_size = HEADS // KV_HEADS
    tokens_wide = tokens.astype(jnp.float32)
    normed = rms_scale(tokens_wide, norm_gain).astype(jnp.bfloat16)
    queries = jnp.dot(normed, query_weight, preferred_element_type=jnp.float32).astype(jnp.bfloat16)
    queries = queries.reshape(seq_count, local_kv, group_size, 2, DQK)
    new_keys = jnp.dot(normed, key_weight, preferred_element_type=jnp.float32).astype(jnp.bfloat16)
    new_keys = new_keys.reshape(seq_count, local_kv, 2, DQK)
    new_values = jnp.dot(normed, value_weight, preferred_element_type=jnp.float32).astype(
        jnp.bfloat16
    )
    new_values = new_values.reshape(seq_count, local_kv, DV)
    key_rows = key_cache.reshape(seq_count, cache_len, local_kv, 2, DQK)
    score_scale = DQK ** (-0.5)
    cache_scores = (
        jnp.einsum("skgmd,sckmd->skgmc", queries, key_rows, preferred_element_type=jnp.float32)
        * score_scale
    )
    own_score = (
        jnp.einsum("skgmd,skmd->skgm", queries, new_keys, preferred_element_type=jnp.float32)
        * score_scale
    )
    live_mask = jnp.arange(cache_len)[None, :] < lengths[:, None]
    cache_scores = jnp.where(live_mask[:, None, None, None, :], cache_scores, -jnp.inf)
    top_score = jnp.maximum(jnp.max(cache_scores, axis=-1), own_score)
    cache_exp = jnp.exp(cache_scores - top_score[..., None])
    own_exp = jnp.exp(own_score - top_score)
    totals = jnp.sum(cache_exp, axis=-1) + own_exp
    cache_prob = cache_exp / totals[..., None]
    own_prob = own_exp / totals
    lambda_grid = lambdas.reshape(local_kv, group_size)
    cache_weight = (
        cache_prob[:, :, :, 0] - lambda_grid[None, :, :, None] * cache_prob[:, :, :, 1]
    ).astype(jnp.bfloat16)
    own_weight = (own_prob[..., 0] - lambda_grid[None] * own_prob[..., 1]).astype(jnp.bfloat16)
    mixture = jnp.einsum(
        "skgc,sckv->skgv", cache_weight, value_cache, preferred_element_type=jnp.float32
    )
    mixture = (
        mixture
        + own_weight.astype(jnp.float32)[..., None] * new_values.astype(jnp.float32)[:, :, None, :]
    )
    head_rows = rms_scale(mixture, head_gain).astype(jnp.bfloat16).reshape(seq_count, -1)
    partial_value = jnp.dot(head_rows, output_weight, preferred_element_type=jnp.float32)
    attention = taken_together(partial_value.astype(jnp.bfloat16), "tp").astype(jnp.float32)
    residual = tokens_wide + attention
    ffn_in = rms_scale(residual, ffn_gain).astype(jnp.bfloat16)
    contract = (((1,), (1,)), ((), ()))
    gate_pre = lax.dot_general(ffn_in, dense_gate, contract, preferred_element_type=jnp.float32)
    up_proj = lax.dot_general(ffn_in, dense_up, contract, preferred_element_type=jnp.float32)
    dense_hidden = (jax.nn.silu(gate_pre) * up_proj).astype(jnp.bfloat16)
    logit_part = jnp.sum(dense_hidden.astype(jnp.float32) * gate_vector, axis=-1)
    dense_term = jnp.dot(dense_hidden, dense_down, preferred_element_type=jnp.float32)
    gate_logit = of_everyone(logit_part, "tp")
    dense_sum = sent_and_summed(dense_term.astype(jnp.bfloat16), "tp", 1)
    dense_out = jax.nn.sigmoid(gate_logit)[:, None] * dense_sum
    experts_total = lax.axis_size("ep")
    capacity = max(2, 2 * seq_count * TOPK // experts_total)
    slot_total = experts_total * capacity
    pair_expert = routes.reshape(-1)
    onehot = (pair_expert[:, None] == jnp.arange(experts_total, dtype=jnp.int32)[None, :]).astype(
        jnp.int32
    )
    slot_rank = jnp.sum(jnp.cumsum(onehot, axis=0) * onehot, axis=1) - 1
    slot_index = pair_expert * capacity + slot_rank
    dispatch = jnp.sum(
        slot_index.reshape(seq_count, TOPK)[None, :, :]
        == jnp.arange(slot_total, dtype=jnp.int32)[:, None, None],
        axis=2,
    )
    outbound = jnp.dot(dispatch.astype(jnp.bfloat16), ffn_in, preferred_element_type=jnp.float32)
    outbound = outbound.astype(jnp.bfloat16).reshape(experts_total, capacity, model_width)
    arrived = lax.all_to_all(outbound, "ep", split_axis=0, concat_axis=0, tiled=True)
    sources, items, width = arrived.shape
    hidden_rows = expert_hidden_rows(arrived.reshape(-1, width), expert_gate, expert_up)
    expert_part = jnp.dot(hidden_rows, expert_down[0], preferred_element_type=jnp.float32)
    expert_part = expert_part.reshape(sources, items, width)
    summed = sent_and_summed(expert_part.astype(jnp.bfloat16), "tp", 2).astype(jnp.bfloat16)
    returned = lax.all_to_all(summed, "ep", split_axis=0, concat_axis=0, tiled=True)
    flat_back = returned.reshape(slot_total, -1)
    picked = flat_back[slot_index].reshape(seq_count, TOPK, -1).astype(jnp.float32)
    expert_mix = jnp.sum(picked * route_weight[:, :, None], axis=1)
    own_columns = model_width // lax.axis_size("tp")
    residual_part = lax.dynamic_slice_in_dim(
        residual, lax.axis_index("tp") * own_columns, own_columns, 1
    )
    return (residual_part + expert_mix + dense_out).astype(jnp.bfloat16)


def solution(mesh):
    placed = (
        P("ep", None),
        P(),
        P(None, "tp"),
        P(None, "tp"),
        P(None, "tp"),
        P("tp", None),
        P(),
        P("tp"),
        P("ep", None, "tp", None),
        P("ep", None, "tp", None),
        P("ep"),
        P(),
        P("ep", None),
        P("ep", None),
        P("ep", None, "tp"),
        P("ep", None, "tp"),
        P("ep", "tp", None),
        P("tp", None),
        P("tp", None),
        P("tp", None),
        P("tp"),
    )
    return jax.shard_map(
        shards, mesh=mesh, in_specs=placed, out_specs=P("ep", "tp"), check_vma=False
    )
```

profile of v0, /device:TPU:1, one launch (start us, length us, event | category | flops | bytes accessed | tf_op | source)
XLA Modules:
  0.0 114.0 jit_solution(5457715531044594561)
XLA Ops:
  0.0 1.1 fusion.17
  1.1 1.6 %convolution_convert_fusion.4 = bf16[16,256]{1,0:T(8,128)(2,1)S(1)} fusion(bf16[2048,256]{1,0:T(8,128)(2,1)} %param.23, bf16[16,2048]{1,0:T(8,128)(2,1)} %param.21, f32[2048]{0:T(1024)} %param.22, f32[16]{0:T(128)S(1)} %add_rsqrt_fusion.2), kind=kOutput, calls=%fused_computation.16 | convolution fusion | flops 16912384 | bytes 1130560 | tf_op jit(solution)/shard_map/dot_general | solution.py:83
  2.8 1.3 %convolution_convert_fusion.6 = bf16[16,128]{1,0:T(8,128)(2,1)S(1)} fusion(bf16[2048,128]{1,0:T(8,128)(2,1)} %param.24, bf16[16,2048]{1,0:T(8,128)(2,1)} %param.21, f32[2048]{0:T(1024)} %param.22, f32[16]{0:T(128)S(1)} %add_rsqrt_fusion.2), kind=kOutput, calls=%fused_computation.19 | convolution fusion | flops 8521728 | bytes 602176 | tf_op jit(solution)/shard_map/dot_general | solution.py:85
  4.5 6.4 %copy.96 = bf16[16,1024,1,128]{1,3,0,2:T(8,128)(2,1)} copy(bf16[16,1024,1,128]{3,1,2,0:T(8,128)(2,1)} %param.29) | data formatting | bytes 8388608 | tf_op args[8]
  11.0 3.0 %fusion.43 = (f32[16,2,2]{1,2,0:T(2,128)S(1)}, f32[16,1,2,2,1024]{4,2,3,0,1:T(2,128)S(1)}) fusion(bf16[16,1024,2,64]{1,3,2,0:T(8,128)(2,1)} %bitcast.128, bf16[16,2,2,64]{3,2,1,0:T(2,128)(2,1)S(1)} %reshape.216, pred[16,1024]{1,0:T(8,128)(4,1)S(1)} %iota_compare_fusion), kind=kOutput, calls=%fused_computation.85 | convolution fusion | flops 8585152 | bytes 4481280 | tf_op jit(solution)/shard_map/skgmd,sckmd->skgmc/dot_general | solution.py:94
  15.5 3.1 %multiply_reduce_fusion.3 = (f32[16,2]{1,0:T(8,128)S(1)}, f32[16,2,128]{2,1,0:T(2,128)S(1)}) fusion(f32[16,128]{1,0:T(8,128)S(1)} %fusion.10, f32[16,2]{1,0:T(8,128)S(1)} %copy.104, bf16[16,1024,1,128]{3,1,2,0:T(8,128)(2,1)} %param.30, f32[16,1,2,2,1024]{4,2,3,0,1:T(2,128)S(1)} %fusion.15, f32[2]{0:T(128)S(1)} %copy-done.7), kind=kOutput, calls=%fused_computation.55 | convolution fusion | flops 8503264 | bytes 4481288 | tf_op jit(solution)/shard_map/skgc,sckv->skgv/dot_general | solution.py:114
  19.7 4.8 %all-to-all-start = ((bf16[4,16,2048]{2,1,0:T(8,128)(2,1)}), bf16[4,16,2048]{2,1,0:T(8,128)(2,1)S(1)}, u32[]{:S(2)}, u32[]{:S(2)}) async-start(bf16[4,16,2048]{2,1,0:T(8,128)(2,1)} %broadcast_in_dim.18), calls=%async_computation | async-start | bytes 524288 | tf_op jit(solution)/shard_map/all_to_all | solution.py:18
  25.3 4.7 %all-to-all-done = bf16[4,16,2048]{2,1,0:T(8,128)(2,1)S(1)} async-done(((bf16[4,16,2048]{2,1,0:T(8,128)(2,1)}), bf16[4,16,2048]{2,1,0:T(8,128)(2,1)S(1)}, u32[]{:S(2)}, u32[]{:S(2)}) %all-to-all-start) | async-done | bytes 262176 | tf_op jit(solution)/shard_map/all_to_all | solution.py:18
  30.7 1.1 reshape.221
  31.8 13.8 %all-to-all-start.1 = ((bf16[64,2,2048]{2,1,0:T(2,128)(2,1)}), bf16[64,2,2048]{2,1,0:T(2,128)(2,1)S(1)}, u32[]{:S(2)}, u32[]{:S(2)}) async-start(bf16[64,2,2048]{2,1,0:T(2,128)(2,1)} %reshape.221), calls=%async_computation.1 | async-start | bytes 1048576 | tf_op jit(solution)/shard_map/all_to_all | solution.py:151
  45.6 2.4 %fusion.44 = f32[16,512]{1,0:T(8,128)S(1)} fusion(bf16[16,2048]{1,0:T(8,128)(2,1)S(1)} %multiply_convert_fusion, bf16[512,2048]{1,0:T(8,128)(2,1)} %param.38), kind=kOutput, calls=%fused_computation.86 | convolution fusion | flops 33554432 | bytes 2195456 | tf_op jit(solution)/shard_map/dot_general | solution.py:127
  48.8 14.4 %all-to-all-done.1 = bf16[64,2,2048]{2,1,0:T(2,128)(2,1)S(1)} async-done(((bf16[64,2,2048]{2,1,0:T(2,128)(2,1)}), bf16[64,2,2048]{2,1,0:T(2,128)(2,1)S(1)}, u32[]{:S(2)}, u32[]{:S(2)}) %all-to-all-start.1) | async-done | bytes 524320 | tf_op jit(solution)/shard_map/all_to_all | solution.py:151
  63.8 3.2 %all-to-all-start.4 = ((f32[4,1,16]{2,1,0:T(1,128)}), f32[4,1,16]{2,1,0:T(1,128)S(1)}, u32[]{:S(2)}, u32[]{:S(2)}) async-start(f32[4,1,16]{2,1,0:T(1,128)} %broadcast_in_dim.19), calls=%async_computation.4 | async-start | bytes 4096 | tf_op jit(solution)/shard_map/all_to_all | solution.py:18
  67.3 1.5 %fusion.13 = f32[128,256]{1,0:T(8,128)S(1)} fusion(bf16[128,2048]{1,0:T(8,128)(2,1)S(1)} %reshape.222, bf16[1,2048,256]{2,1,0:T(8,128)(2,1)} %param.35), kind=kOutput, calls=%fused_computation.22 | convolution fusion | flops 134217728 | bytes 1703936 | tf_op jit(solution)/shard_map/dot_general | solution.py:48
  68.8 1.5 %fusion.5 = bf16[128,256]{1,0:T(8,128)(2,1)S(1)} fusion(bf16[128,2048]{1,0:T(8,128)(2,1)S(1)} %reshape.222, bf16[1,2048,256]{2,1,0:T(8,128)(2,1)} %param.36, f32[128,256]{1,0:T(8,128)S(1)} %fusion.13), kind=kOutput, calls=%fused_computation.12 | convolution fusion | flops 134414336 | bytes 1769472 | tf_op jit(solution)/shard_map/dot_general | solution.py:49
  70.4 1.5 %convolution_convert_fusion = bf16[64,2,2048]{2,0,1:T(8,128)(2,1)S(1)} fusion(bf16[1,256,2048]{2,1,0:T(8,128)(2,1)} %param.37, bf16[64,2,256]{2,1,0:T(2,128)(2,1)S(1)} %dot_general.54), kind=kOutput, calls=%fused_computation.3 | convolution fusion | flops 134479872 | bytes 1638400 | tf_op jit(solution)/shard_map/dot_general | solution.py:154
  71.9 0.8 copy.142
  72.8 4.2 %all-to-all-start.2 = ((bf16[4,64,2,512]{3,1,2,0:T(8,128)(2,1)}), bf16[4,64,2,512]{3,1,2,0:T(8,128)(2,1)S(1)}, u32[]{:S(2)}, u32[]{:S(2)}) async-start(bf16[4,64,2,512]{3,1,2,0:T(8,128)(2,1)} %bitcast.125), calls=%async_computation.2 | async-start | bytes 1048576 | tf_op jit(solution)/shard_map/all_to_all | solution.py:39
  78.0 7.3 %all-to-all-done.2 = bf16[4,64,2,512]{3,1,2,0:T(8,128)(2,1)S(1)} async-done(((bf16[4,64,2,512]{3,1,2,0:T(8,128)(2,1)}), bf16[4,64,2,512]{3,1,2,0:T(8,128)(2,1)S(1)}, u32[]{:S(2)}, u32[]{:S(2)}) %all-to-all-start.2) | async-done | bytes 524320 | tf_op jit(solution)/shard_map/all_to_all | solution.py:39
  85.3 3.3 %all-to-all-start.5 = ((bf16[4,16,512]{2,1,0:T(8,128)(2,1)}), bf16[4,16,512]{2,1,0:T(8,128)(2,1)S(1)}, u32[]{:S(2)}, u32[]{:S(2)}) async-start(bf16[4,16,512]{2,1,0:T(8,128)(2,1)} %bitcast.127), calls=%async_computation.5 | async-start | bytes 131072 | tf_op jit(solution)/shard_map/all_to_all | solution.py:39
  88.8 0.8 copy.111
  89.6 3.5 %all-to-all-done.5 = bf16[4,16,512]{2,1,0:T(8,128)(2,1)S(1)} async-done(((bf16[4,16,512]{2,1,0:T(8,128)(2,1)}), bf16[4,16,512]{2,1,0:T(8,128)(2,1)S(1)}, u32[]{:S(2)}, u32[]{:S(2)}) %all-to-all-start.5) | async-done | bytes 65568 | tf_op jit(solution)/shard_map/all_to_all | solution.py:39
  93.0 8.2 %all-to-all-start.3 = ((bf16[64,2,512]{2,1,0:T(2,128)(2,1)}), bf16[64,2,512]{2,1,0:T(2,128)(2,1)S(1)}, u32[]{:S(2)}, u32[]{:S(2)}) async-start(bf16[64,2,512]{2,1,0:T(2,128)(2,1)} %copy.111), calls=%async_computation.3 | async-start | bytes 262144 | tf_op jit(solution)/shard_map/all_to_all | solution.py:157
  101.3 11.1 %all-to-all-done.3 = bf16[64,2,512]{2,1,0:T(2,128)(2,1)S(1)} async-done(((bf16[64,2,512]{2,1,0:T(2,128)(2,1)}), bf16[64,2,512]{2,1,0:T(2,128)(2,1)S(1)}, u32[]{:S(2)}, u32[]{:S(2)}) %all-to-all-start.3) | async-done | bytes 131104 | tf_op jit(solution)/shard_map/all_to_all | solution.py:157
  (83 shorter events, 9.0 us)
Async XLA Ops:
  0.0 77.0 %copy-start = (bf16[512,2048]{1,0:T(8,128)(2,1)S(1)}, bf16[512,2048]{1,0:T(8,128)(2,1)}, u32[]{:S(2)}) copy-start(bf16[512,2048]{1,0:T(8,128)(2,1)} %param.40) | copy-start | bytes 6291460
  4.5 6.4 %copy-start.12 = (s32[16]{0:T(128)S(1)}, s32[16]{0:T(128)}, u32[]{:S(2)}) copy-start(s32[16]{0:T(128)} %param.31) | copy-start | bytes 196
  11.0 4.1 %copy-start.7 = (f32[2]{0:T(128)S(1)}, f32[2]{0:T(128)}, u32[]{:S(2)}) copy-start(f32[2]{0:T(128)} %param.28) | copy-start | bytes 28
  11.0 4.3 %copy-start.2 = (bf16[16,2048]{1,0:T(8,128)(2,1)S(1)}, bf16[16,2048]{1,0:T(8,128)(2,1)}, u32[]{:S(2)}) copy-start(bf16[16,2048]{1,0:T(8,128)(2,1)} %param.21) | copy-start | bytes 196612
  11.0 4.3 %copy-start.4 = (bf16[2048,128]{1,0:T(8,128)(2,1)S(1)}, bf16[2048,128]{1,0:T(8,128)(2,1)}, u32[]{:S(2)}) copy-start(bf16[2048,128]{1,0:T(8,128)(2,1)} %param.25) | copy-start | bytes 1572868
  11.0 4.2 %copy-start.5 = (f32[2048]{0:T(1024)S(1)}, f32[2048]{0:T(1024)}, u32[]{:S(2)}) copy-start(f32[2048]{0:T(1024)} %param.22) | copy-start | bytes 24580
  15.5 3.1 %copy-start.11 = (f32[128]{0:T(128)S(1)}, f32[128]{0:T(128)}, u32[]{:S(2)}) copy-start(f32[128]{0:T(128)} %param.27) | copy-start | bytes 1540
  15.5 3.2 %copy-start.3 = (bf16[256,2048]{1,0:T(8,128)(2,1)S(1)}, bf16[256,2048]{1,0:T(8,128)(2,1)}, u32[]{:S(2)}) copy-start(bf16[256,2048]{1,0:T(8,128)(2,1)} %param.26) | copy-start | bytes 3145732
  15.5 9.0 %copy-start.8 = (s32[16,4]{0,1:T(4,128)S(1)}, s32[16,4]{0,1:T(4,128)}, u32[]{:S(2)}) copy-start(s32[16,4]{0,1:T(4,128)} %param.33) | copy-start | bytes 772
  18.6 11.6 %copy-start.6 = (f32[2048]{0:T(1024)S(1)}, f32[2048]{0:T(1024)}, u32[]{:S(2)}) copy-start(f32[2048]{0:T(1024)} %param.32) | copy-start | bytes 24580
  19.7 10.4 %all-to-all-start = ((bf16[4,16,2048]{2,1,0:T(8,128)(2,1)}), bf16[4,16,2048]{2,1,0:T(8,128)(2,1)S(1)}, u32[]{:S(2)}, u32[]{:S(2)}) async-start(bf16[4,16,2048]{2,1,0:T(8,128)(2,1)} %broadcast_in_dim.18), calls=%async_computation | async-start | bytes 524288 | tf_op jit(solution)/shard_map/all_to_all | solution.py:18
  30.6 17.4 %copy-start.10 = (f32[512]{0:T(512)S(1)}, f32[512]{0:T(512)}, u32[]{:S(2)}) copy-start(f32[512]{0:T(512)} %param.41) | copy-start | bytes 6148
  31.8 31.5 %all-to-all-start.1 = ((bf16[64,2,2048]{2,1,0:T(2,128)(2,1)}), bf16[64,2,2048]{2,1,0:T(2,128)(2,1)S(1)}, u32[]{:S(2)}, u32[]{:S(2)}) async-start(bf16[64,2,2048]{2,1,0:T(2,128)(2,1)} %reshape.221), calls=%async_computation.1 | async-start | bytes 1048576 | tf_op jit(solution)/shard_map/all_to_all | solution.py:151
  45.6 2.4 %copy-start.1 = (bf16[512,2048]{1,0:T(8,128)(2,1)S(1)}, bf16[512,2048]{1,0:T(8,128)(2,1)}, u32[]{:S(2)}) copy-start(bf16[512,2048]{1,0:T(8,128)(2,1)} %param.39) | copy-start | bytes 6291460
  63.8 9.0 %all-to-all-start.4 = ((f32[4,1,16]{2,1,0:T(1,128)}), f32[4,1,16]{2,1,0:T(1,128)S(1)}, u32[]{:S(2)}, u32[]{:S(2)}) async-start(f32[4,1,16]{2,1,0:T(1,128)} %broadcast_in_dim.19), calls=%async_computation.4 | async-start | bytes 4096 | tf_op jit(solution)/shard_map/all_to_all | solution.py:18
  71.9 16.7 %copy-start.9 = (f32[16,4]{0,1:T(4,128)S(1)}, f32[16,4]{0,1:T(4,128)}, u32[]{:S(2)}) copy-start(f32[16,4]{0,1:T(4,128)} %param.34) | copy-start | bytes 772
  72.8 12.5 %all-to-all-start.2 = ((bf16[4,64,2,512]{3,1,2,0:T(8,128)(2,1)}), bf16[4,64,2,512]{3,1,2,0:T(8,128)(2,1)S(1)}, u32[]{:S(2)}, u32[]{:S(2)}) async-start(bf16[4,64,2,512]{3,1,2,0:T(8,128)(2,1)} %bitcast.125), calls=%async_computation.2 | async-start | bytes 1048576 | tf_op jit(solution)/shard_map/all_to_all | solution.py:39
  85.3 7.7 %all-to-all-start.5 = ((bf16[4,16,512]{2,1,0:T(8,128)(2,1)}), bf16[4,16,512]{2,1,0:T(8,128)(2,1)S(1)}, u32[]{:S(2)}, u32[]{:S(2)}) async-start(bf16[4,16,512]{2,1,0:T(8,128)(2,1)} %bitcast.127), calls=%async_computation.5 | async-start | bytes 131072 | tf_op jit(solution)/shard_map/all_to_all | solution.py:39
  93.0 19.3 %all-to-all-start.3 = ((bf16[64,2,512]{2,1,0:T(2,128)(2,1)}), bf16[64,2,512]{2,1,0:T(2,128)(2,1)S(1)}, u32[]{:S(2)}, u32[]{:S(2)}) async-start(bf16[64,2,512]{2,1,0:T(2,128)(2,1)} %copy.111), calls=%async_computation.3 | async-start | bytes 262144 | tf_op jit(solution)/shard_map/all_to_all | solution.py:157
where the time goes:
time: 115 us; the launch traced here: 114 us
  waiting for transfers between devices  41 us (36%)
  starting transfers between devices  37.5 us (33%)
  matrix products  18.1 us (16%)
  local copies, waits for them, and re-layouts  13.4 us (12%)
  other arithmetic  3.7 us (3%)
    all_to_all x1, waiting for transfers between devices, shards(): lax.all_to_all(outbound, 'ep', split_axis=0, concat_axis=0, tiled=True)  14.4 us
    all_to_all x1, starting transfers between devices, shards(): lax.all_to_all(outbound, 'ep', split_axis=0, concat_axis=0, tiled=True)  13.8 us
    all_to_all x1, waiting for transfers between devices, shards(): lax.all_to_all(summed, 'ep', split_axis=0, concat_axis=0, tiled=True)  11.1 us
    all_to_all x2, waiting for transfers between devices, sent_and_summed(): lax.all_to_all(cut_along(shard, dim, devices), axis, 0, 0, tiled=True)  10.8 us
    all_to_all x1, starting transfers between devices, shards(): lax.all_to_all(summed, 'ep', split_axis=0, concat_axis=0, tiled=True)  8.19 us
    all_to_all x2, starting transfers between devices, from_everyone(): lax.all_to_all(jnp.broadcast_to(shard[None], (devices, *shard.shape)), ax...  8.05 us
    all_to_all x2, starting transfers between devices, sent_and_summed(): lax.all_to_all(cut_along(shard, dim, devices), axis, 0, 0, tiled=True)  7.48 us
    unnamed x29, local copies, waits for them, and re-layouts  6.66 us
  transfers between devices with their start and end apart: 6, of which 5 were waited for; matrix products, arithmetic and copies ran while one was open for 10% of the time, Pallas kernels for 0%

commit v1 on v0

v1 whole, which is shorter than its diff:
```python
import jax
import jax.numpy as jnp
from jax import lax
from jax.experimental import pallas as pl
from jax.experimental.pallas import tpu as pltpu
from jax.sharding import PartitionSpec as P

HEADS = 8
KV_HEADS = 4
DQK = 64
DV = 128
TOPK = 4
CAP = 2
GROUP = 4

epsilon = 1e-06
F32 = jnp.float32
BF16 = jnp.bfloat16


def rms_scale(values, gain):
    return values * lax.rsqrt(jnp.mean(values * values, axis=-1, keepdims=True) + epsilon) * gain


def dot(lhs, rhs, contract=((1,), (0,))):
    return lax.dot_general(lhs, rhs, (contract, ((), ())), preferred_element_type=F32)


def attention_kernel(
    lengths,
    lambdas,
    tokens,
    norm_gain,
    head_gain,
    routes,
    route_weight,
    query_hbm,
    key_hbm,
    value_hbm,
    output_hbm,
    key_cache,
    value_cache,
    partial_out,
    dispatch_out,
    mix_out,
    query_weight,
    key_weight,
    value_weight,
    output_weight,
    keys,
    values,
    mixture,
    sems,
):
    seq_count = tokens.shape[0]
    groups = seq_count // GROUP
    copies = [
        pltpu.make_async_copy(query_hbm, query_weight, sems.at[0]),
        pltpu.make_async_copy(key_hbm, key_weight, sems.at[1]),
        pltpu.make_async_copy(value_hbm, value_weight, sems.at[2]),
    ]
    for group in range(groups):
        rows = pl.ds(group * GROUP, GROUP)
        copies.append(
            pltpu.make_async_copy(key_cache.at[rows], keys.at[rows], sems.at[4 + 2 * group])
        )
        copies.append(
            pltpu.make_async_copy(value_cache.at[rows], values.at[rows], sems.at[5 + 2 * group])
        )
    last = pltpu.make_async_copy(output_hbm, output_weight, sems.at[3])
    for copy in copies:
        copy.start()
    last.start()

    slots = dispatch_out.shape[0]
    slot_ids = lax.broadcasted_iota(jnp.int32, (slots, seq_count), 0)
    named = jnp.zeros((slots, seq_count), F32)
    weighed = jnp.zeros((slots, seq_count), F32)
    for k in range(TOPK):
        hit = (slot_ids // CAP) == routes[k : k + 1, :]
        named = named + jnp.where(hit, 1.0, 0.0)
        weighed = weighed + jnp.where(hit, route_weight[k : k + 1, :], 0.0)
    before = lax.broadcasted_iota(jnp.int32, (seq_count, seq_count), 0)
    after = lax.broadcasted_iota(jnp.int32, (seq_count, seq_count), 1)
    earlier = jnp.where(before < after, 1.0, 0.0).astype(BF16)
    rank = dot(named.astype(BF16), earlier)
    chosen = rank == (slot_ids % CAP).astype(F32)
    dispatch_out[...] = jnp.where(chosen, named, 0.0).astype(BF16)
    mix_out[...] = jnp.where(chosen, weighed, 0.0)

    normed = rms_scale(tokens[...].astype(F32), norm_gain[...]).astype(BF16)
    copies[0].wait()
    queries = dot(normed, query_weight[...]).astype(BF16).astype(F32)
    copies[1].wait()
    new_keys = dot(normed, key_weight[...]).astype(BF16).astype(F32)
    copies[2].wait()
    new_values = dot(normed, value_weight[...]).astype(BF16).astype(F32)

    cache_len = keys.shape[1]
    row = lax.broadcasted_iota(jnp.int32, (8, 2 * DQK), 0)
    lane = lax.broadcasted_iota(jnp.int32, (8, 2 * DQK), 1)
    keep = jnp.logical_and((lane // DQK) == (row % 2), row < 4)
    row1 = lax.broadcasted_iota(jnp.int32, (8, 1), 0)
    sign = jnp.where(row1 % 2 == 0, 1.0, -jnp.where(row1 < 2, lambdas[0], lambdas[1]))
    position = lax.broadcasted_iota(jnp.int32, (8, cache_len), 1)
    score_scale = DQK ** (-0.5)
    for group in range(groups):
        copies[3 + 2 * group].wait()
        scores = []
        own_scores = []
        for s in range(group * GROUP, (group + 1) * GROUP):
            first = jnp.broadcast_to(queries[s : s + 1, : 2 * DQK], (8, 2 * DQK))
            second = jnp.broadcast_to(queries[s : s + 1, 2 * DQK :], (8, 2 * DQK))
            query = jnp.where(keep, jnp.where(row < 2, first, second), 0.0)
            score = dot(query.astype(BF16), keys[s], ((1,), (1,))) * score_scale
            scores.append(jnp.where(position < lengths[s], score, -jnp.inf))
            own_scores.append(
                jnp.sum(query * new_keys[s : s + 1, :], axis=1, keepdims=True) * score_scale
            )
        weights = []
        own_weights = []
        for score, own in zip(scores, own_scores):
            top = jnp.maximum(jnp.max(score, axis=1, keepdims=True), own)
            grown = jnp.exp(score - top)
            own_grown = jnp.exp(own - top)
            total = jnp.sum(grown, axis=1, keepdims=True) + own_grown
            share = sign / total
            prob = grown * share
            own_prob = own_grown * share
            weights.append((prob + pltpu.roll(prob, 7, 0)).astype(BF16))
            own_weights.append((own_prob + pltpu.roll(own_prob, 7, 0)).astype(BF16).astype(F32))
        copies[4 + 2 * group].wait()
        for i in range(GROUP):
            s = group * GROUP + i
            mixed = dot(weights[i], values[s]) + own_weights[i] * new_values[s : s + 1, :]
            mixture[s : s + 1, :DV] = mixed[0:1, :]
            mixture[s : s + 1, DV:] = mixed[2:3, :]
    gain = head_gain[...]
    left = rms_scale(mixture[:, :DV], gain).astype(BF16)
    right = rms_scale(mixture[:, DV:], gain).astype(BF16)
    last.wait()
    result = dot(left, output_weight[:DV, :]) + dot(right, output_weight[DV:, :])
    partial_out[...] = result.astype(BF16)


def whole(count):
    return [pl.BlockSpec(memory_space=pltpu.VMEM)] * count


def attend(tokens, norm_gain, query_weight, key_weight, value_weight, output_weight, head_gain,
           lambdas, key_cache, value_cache, lengths, routes, route_weight, slots):
    seq_count, width = tokens.shape
    smem = pl.BlockSpec(memory_space=pltpu.SMEM)
    hbm = pl.BlockSpec(memory_space=pl.ANY)
    groups = seq_count // GROUP
    return pl.pallas_call(
        attention_kernel,
        name="attend",
        out_shape=(
            jax.ShapeDtypeStruct((seq_count, width), BF16),
            jax.ShapeDtypeStruct((slots, seq_count), BF16),
            jax.ShapeDtypeStruct((slots, seq_count), F32),
        ),
        in_specs=[smem, smem] + whole(5) + [hbm] * 6,
        out_specs=tuple(whole(3)),
        scratch_shapes=[
            pltpu.VMEM(query_weight.shape, BF16),
            pltpu.VMEM(key_weight.shape, BF16),
            pltpu.VMEM(value_weight.shape, BF16),
            pltpu.VMEM(output_weight.shape, BF16),
            pltpu.VMEM(key_cache.shape, BF16),
            pltpu.VMEM(value_cache.shape, BF16),
            pltpu.VMEM((seq_count, 2 * DV), F32),
            pltpu.SemaphoreType.DMA((4 + 2 * groups,)),
        ],
    )(lengths, lambdas, tokens, norm_gain, head_gain, routes, route_weight,
      query_weight, key_weight, value_weight, output_weight, key_cache, value_cache)


def normalise_kernel(tokens, own, one, two, three, gain, dispatch, residual, ffn_in, outbound):
    attention = (own[...].astype(F32) + one[...].astype(F32)) + (
        two[...].astype(F32) + three[...].astype(F32)
    )
    total = tokens[...].astype(F32) + attention
    residual[...] = total
    rows = rms_scale(total, gain[...]).astype(BF16)
    ffn_in[...] = rows
    outbound[...] = dot(dispatch[...], rows).astype(BF16)


def normalise(tokens, parts, gain, dispatch):
    seq_count, width = tokens.shape
    return pl.pallas_call(
        normalise_kernel,
        name="normalise",
        out_shape=(
            jax.ShapeDtypeStruct((seq_count, width), F32),
            jax.ShapeDtypeStruct((seq_count, width), BF16),
            jax.ShapeDtypeStruct((dispatch.shape[0], width), BF16),
        ),
        in_specs=whole(7),
        out_specs=tuple(whole(3)),
    )(tokens, *parts, gain, dispatch)


def silu(values):
    return values / (1.0 + jnp.exp(-values))


def dense_kernel(rows, gate, up, down, vector, term, logit):
    value = rows[...]
    gate_pre = dot(value, gate[...], ((1,), (1,)))
    up_proj = dot(value, up[...], ((1,), (1,)))
    hidden = (silu(gate_pre) * up_proj).astype(BF16)
    term[...] = dot(hidden, down[...]).astype(BF16)
    part = jnp.sum(hidden.astype(F32) * vector[...], axis=1, keepdims=True)
    high = part.astype(BF16)
    rest = part - high.astype(F32)
    middle = rest.astype(BF16)
    low = (rest - middle.astype(F32)).astype(BF16)
    lane = lax.broadcasted_iota(jnp.int32, logit.shape, 1)
    pieces = jnp.where(
        lane == 0, high.astype(F32), jnp.where(lane == 1, middle.astype(F32), low.astype(F32))
    )
    logit[...] = jnp.where(lane < 3, pieces, 0.0).astype(BF16)


def dense_branch(rows, gate, up, down, vector, columns):
    seq_count, width = rows.shape
    return pl.pallas_call(
        dense_kernel,
        name="dense",
        out_shape=(
            jax.ShapeDtypeStruct((seq_count, width), BF16),
            jax.ShapeDtypeStruct((seq_count, columns), BF16),
        ),
        in_specs=whole(5),
        out_specs=tuple(whole(2)),
        cost_estimate=pl.CostEstimate(
            flops=6 * seq_count * width * gate.shape[0],
            bytes_accessed=6 * width * gate.shape[0],
            transcendentals=0,
        ),
    )(rows, gate, up, down, vector)


def expert_kernel(place, rows, gate, up, down, term, logit, *blocks):
    value = rows[...]
    hidden = (silu(dot(value, gate[...])) * dot(value, up[...])).astype(BF16)
    count, columns = value.shape[0], blocks[0].shape[1]
    seq_count = term.shape[0]
    for step, block in enumerate(blocks):
        start = pl.multiple_of(((place[0] + step) % len(blocks)) * columns, columns)
        block[:count, :] = dot(hidden, down[:, pl.ds(start, columns)]).astype(BF16)
        block[count : count + seq_count, :] = term[:, pl.ds(start, columns)]
        block[count + seq_count :, :] = logit[...]


def expert_rows(place, rows, gate, up, down, term, logit, devices):
    count, width = rows.shape
    seq_count, columns = logit.shape
    shape = jax.ShapeDtypeStruct((count + 2 * seq_count, columns), BF16)
    return pl.pallas_call(
        expert_kernel,
        name="experts",
        out_shape=(shape,) * devices,
        in_specs=[pl.BlockSpec(memory_space=pltpu.SMEM)] + whole(6),
        out_specs=tuple(whole(devices)),
    )(place, rows, gate, up, down, term, logit)


def gather_kernel(place, own, one, two, three, residual, summed, kept):
    count, columns = summed.shape
    seq_count = residual.shape[0]
    total = (own[...].astype(F32) + one[...].astype(F32)) + (
        two[...].astype(F32) + three[...].astype(F32)
    )
    summed[...] = total[:count, :].astype(BF16)
    pieces = total[count + seq_count :, :]
    lane = lax.broadcasted_iota(jnp.int32, pieces.shape, 1)
    logit = jnp.sum(jnp.where(lane < 3, pieces, 0.0), axis=1, keepdims=True)
    gated = total[count : count + seq_count, :] / (1.0 + jnp.exp(-logit))
    start = pl.multiple_of(place[0] * columns, columns)
    kept[...] = residual[:, pl.ds(start, columns)] + gated


def gather_parts(place, parts, residual, count):
    seq_count = residual.shape[0]
    columns = parts[0].shape[1]
    return pl.pallas_call(
        gather_kernel,
        name="gather",
        out_shape=(
            jax.ShapeDtypeStruct((count, columns), BF16),
            jax.ShapeDtypeStruct((seq_count, columns), F32),
        ),
        in_specs=[pl.BlockSpec(memory_space=pltpu.SMEM)] + whole(5),
        out_specs=tuple(whole(2)),
    )(place, *parts, residual)


def combine_kernel(kept, mix, returned, out):
    picked = lax.dot_general(
        mix[...],
        returned[...].astype(F32),
        (((0,), (0,)), ((), ())),
        precision=lax.Precision.HIGHEST,
        preferred_element_type=F32,
    )
    out[...] = (kept[...] + picked).astype(BF16)


def combine(kept, mix, returned):
    return pl.pallas_call(
        combine_kernel,
        name="combine",
        out_shape=jax.ShapeDtypeStruct(kept.shape, BF16),
        in_specs=whole(3),
        out_specs=whole(1)[0],
    )(kept, mix, returned)


def passed_on(shard, step):
    devices = lax.axis_size("tp")
    return lax.ppermute(shard, "tp", [(i, (i + step) % devices) for i in range(devices)])


def shards(
    tokens,
    norm_gain,
    query_weight,
    key_weight,
    value_weight,
    output_weight,
    head_gain,
    lambdas,
    key_cache,
    value_cache,
    lengths,
    ffn_gain,
    routes,
    route_weight,
    expert_gate,
    expert_up,
    expert_down,
    dense_gate,
    dense_up,
    dense_down,
    gate_vector,
):
    seq_count, width = tokens.shape
    cache_len = key_cache.shape[1]
    devices = lax.axis_size("tp")
    experts_total = lax.axis_size("ep")
    slots = experts_total * CAP
    columns = width // devices
    place = lax.axis_index("tp").astype(jnp.int32).reshape(1)
    keys = jnp.transpose(key_cache, (0, 2, 1, 3)).reshape(seq_count, cache_len, 2 * DQK)
    values = jnp.transpose(value_cache, (0, 2, 1, 3)).reshape(seq_count, cache_len, DV)
    partial, dispatch, mix = attend(
        tokens, norm_gain[None], query_weight, key_weight, value_weight, output_weight,
        head_gain[None], lambdas, keys, values, lengths, routes.T, route_weight.T, slots,
    )
    parts = [partial] + [passed_on(partial, step) for step in range(1, devices)]
    residual, ffn_in, outbound = normalise(tokens, parts, ffn_gain[None], dispatch)
    arrived = lax.all_to_all(
        outbound.reshape(experts_total, CAP, width), "ep", split_axis=0, concat_axis=0, tiled=True
    )
    term, logit = dense_branch(ffn_in, dense_gate, dense_up, dense_down, gate_vector[None], columns)
    blocks = expert_rows(
        place, arrived.reshape(slots, width), expert_gate[0], expert_up[0], expert_down[0],
        term, logit, devices,
    )
    moved = [blocks[0]] + [passed_on(blocks[step], step) for step in range(1, devices)]
    summed, kept = gather_parts(place, moved, residual, slots)
    returned = lax.all_to_all(
        summed.reshape(experts_total, CAP, columns), "ep", split_axis=0, concat_axis=0, tiled=True
    )
    return combine(kept, mix, returned.reshape(slots, columns))


def solution(mesh):
    placed = (
        P("ep", None),
        P(),
        P(None, "tp"),
        P(None, "tp"),
        P(None, "tp"),
        P("tp", None),
        P(),
        P("tp"),
        P("ep", None, "tp", None),
        P("ep", None, "tp", None),
        P("ep"),
        P(),
        P("ep", None),
        P("ep", None),
        P("ep", None, "tp"),
        P("ep", None, "tp"),
        P("ep", "tp", None),
        P("tp", None),
        P("tp", None),
        P("tp", None),
        P("tp"),
    )
    return jax.shard_map(
        shards, mesh=mesh, in_specs=placed, out_specs=P("ep", "tp"), check_vma=False
    )
```

time: 115 us -> 91.9 us (0.80)
  Pallas kernels: 0 us -> 22 us
  matrix products: 18.1 us -> 0 us
  blocking collectives: 0 us -> 17.3 us
  waiting for transfers between devices: 41 us -> 24.6 us
  starting transfers between devices: 37.5 us -> 21.4 us
  local copies, waits for them, and re-layouts: 13.4 us -> 6.17 us
  other arithmetic: 3.7 us -> 0 us
    all_to_all x6 -> x1, waiting for transfers between devices: 41 us -> 12.6 us  [shards(): lax.all_to_all(outbound.reshape(experts_total, CAP, width), 'ep', split_a...]
    all_to_all x6 -> x1, starting transfers between devices: 37.5 us -> 13.8 us  [shards(): lax.all_to_all(outbound.reshape(experts_total, CAP, width), 'ep', split_a...]
    pallas_call x0 -> x6, Pallas kernels: none -> 22 us  [the longest x1 7.43 us: attend(): pl.pallas_call(attention_kernel, name='attend', out_shape=(jax.ShapeDtype...]
    dot_general x14 -> x0, matrix products: 18.1 us -> none  [the longest x1 3.06 us: shards(): jnp.einsum('skgc,sckv->skgv', cache_weight, value_cache, preferred_elemen...]
    all_to_all x0 -> x1, blocking collectives: none -> 17.3 us  [shards(): lax.all_to_all(summed.reshape(experts_total, CAP, columns), 'ep', split_a...]
    ppermute x0 -> x6, waiting for transfers between devices: none -> 12 us  [passed_on(): lax.ppermute(shard, 'tp', [(i, (i + step) % devices) for i in range(devic...]
    ppermute x0 -> x6, starting transfers between devices: none -> 7.62 us  [passed_on(): lax.ppermute(shard, 'tp', [(i, (i + step) % devices) for i in range(devic...]
    unnamed x29 -> x12, local copies, waits for them, and re-layouts: 6.66 us -> 1.3 us
  transfers between devices with their start and end apart: 6 -> 7, of which waited for: 5 -> 6; matrix products, arithmetic and copies ran while one was open for 10% -> 0% of each run, Pallas kernels for 0% -> 6%
where the time goes in v1:
time: 91.9 us; the launch traced here: 91.5 us
  waiting for transfers between devices  24.6 us (27%)
  Pallas kernels  22 us (24%)
  starting transfers between devices  21.4 us (23%)
  blocking collectives  17.3 us (19%)
  local copies, waits for them, and re-layouts  6.17 us (7%)
    all_to_all x1, blocking collectives, shards(): lax.all_to_all(summed.reshape(experts_total, CAP, columns), 'ep', split_a...  17.3 us
    all_to_all x1, starting transfers between devices, shards(): lax.all_to_all(outbound.reshape(experts_total, CAP, width), 'ep', split_a...  13.8 us
    all_to_all x1, waiting for transfers between devices, shards(): lax.all_to_all(outbound.reshape(experts_total, CAP, width), 'ep', split_a...  12.6 us
    ppermute x6, waiting for transfers between devices, passed_on(): lax.ppermute(shard, 'tp', [(i, (i + step) % devices) for i in range(devic...  12 us
    ppermute x6, starting transfers between devices, passed_on(): lax.ppermute(shard, 'tp', [(i, (i + step) % devices) for i in range(devic...  7.62 us
    pallas_call x1, Pallas kernels, attend(): pl.pallas_call(attention_kernel, name='attend', out_shape=(jax.ShapeDtype...  7.43 us
    pallas_call x1, Pallas kernels, dense_branch(): pl.pallas_call(dense_kernel, name='dense', out_shape=(jax.ShapeDtypeStruc...  5.06 us
    pallas_call x1, Pallas kernels, expert_rows(): pl.pallas_call(expert_kernel, name='experts', out_shape=(shape,) * device...  3.52 us
  transfers between devices with their start and end apart: 7, of which 6 were waited for; matrix products, arithmetic and copies ran while one was open for 0% of the time, Pallas kernels for 6%

profile of v1, /device:TPU:1, one launch (start us, length us, event | category | flops | bytes accessed | tf_op | source)
XLA Modules:
  0.0 91.5 jit_solution(6998084911887958572)
XLA Ops:
  0.0 7.4 %attend.1 = (bf16[16,2048]{1,0:T(8,128)(2,1)}, bf16[128,16]{1,0:T(8,128)(2,1)}, f32[128,16]{1,0:T(8,128)}) custom-call(s32[16]{0:T(128)} %lengths.1, f32[2]{0:T(128)} %lambdas.1, bf16[16,2048]{1,0:T(8,128)(2,1)} %tokens.3, f32[1,2048]{1,0:T(1,128)} %bitcast.17, f32[1,128]{1,0:T(1,128)} %bitcast.22, s32[4,16]{1,0:T(4,128)} %bitcast.19, f32[4,16]{1,0:T(4,128)} %bitcast.20, ...), custom_call_target="tpu_custom_call" | custom-call | tf_op jit(solution)/shard_map/attend/pallas_call | solution.py:156
  7.4 3.4 %collective-permute-start.2 = (bf16[16,2048]{1,0:T(8,128)(2,1)}, bf16[16,2048]{1,0:T(8,128)(2,1)S(1)}, u32[]{:S(2)}, u32[]{:S(2)}) collective-permute-start(bf16[16,2048]{1,0:T(8,128)(2,1)} %get-tuple-element.19.own), channel_id=1, source_target_pairs={{0,3},{1,0},{2,1},{3,2},{4,7},{5,4},{6,5},{7,6},{8,11},{9,8},{10,9... | collective-permute-start | bytes 196616 | tf_op jit(solution)/shard_map/ppermute | solution.py:325
  10.8 0.5 collective-permute-start.1
  11.3 0.6 collective-permute-start
  11.9 0.5 collective-permute-done.2.three
  12.5 3.2 %collective-permute-done.1.two = bf16[16,2048]{1,0:T(8,128)(2,1)S(1)} collective-permute-done((bf16[16,2048]{1,0:T(8,128)(2,1)}, bf16[16,2048]{1,0:T(8,128)(2,1)S(1)}, u32[]{:S(2)}, u32[]{:S(2)}) %collective-permute-start.1) | collective-permute-done | bytes 65568 | tf_op jit(solution)/shard_map/ppermute | solution.py:325
  15.7 0.7 collective-permute-done.one
  16.4 0.6 copy-done.5
  17.0 2.2 %normalise.1 = (f32[16,2048]{1,0:T(8,128)}, bf16[16,2048]{1,0:T(8,128)(2,1)}, bf16[128,2048]{1,0:T(8,128)(2,1)}) custom-call(bf16[16,2048]{1,0:T(8,128)(2,1)} %tokens.3, bf16[16,2048]{1,0:T(8,128)(2,1)} %get-tuple-element.19.own, bf16[16,2048]{1,0:T(8,128)(2,1)} %copy-done.5, bf16[16,2048]{1,0:T(8,128)(2,1)} %copy-done.4, bf16[16,2048]{1,0:T(8,128)(2,1)} %copy-done.3, ...), custom_call_target="tpu_custom_call" | custom-call | tf_op jit(solution)/shard_map/normalise/pallas_call | solution.py:193
  19.2 2.2 %reshape.16 = bf16[64,2,2048]{2,1,0:T(2,128)(2,1)} reshape(bf16[128,2048]{1,0:T(8,128)(2,1)} %get-tuple-element.21) | data formatting | bytes 1048576 | tf_op jit(solution)/shard_map/reshape | solution.py:367
  21.4 13.8 %all-to-all-start = ((bf16[64,2,2048]{2,1,0:T(2,128)(2,1)}), bf16[64,2,2048]{2,1,0:T(2,128)(2,1)S(1)}, u32[]{:S(2)}, u32[]{:S(2)}) async-start(bf16[64,2,2048]{2,1,0:T(2,128)(2,1)} %reshape.16), calls=%async_computation | async-start | bytes 1048576 | tf_op jit(solution)/shard_map/all_to_all | solution.py:366
  35.1 5.1 %dense.1 = (bf16[16,2048]{1,0:T(8,128)(2,1)}, bf16[16,512]{1,0:T(8,128)(2,1)}) custom-call(bf16[16,2048]{1,0:T(8,128)(2,1)} %get-tuple-element.22.rows, bf16[512,2048]{1,0:T(8,128)(2,1)} %gate.1, bf16[512,2048]{1,0:T(8,128)(2,1)} %up.1, bf16[512,2048]{1,0:T(8,128)(2,1)} %down.1, f32[1,512]{1,0:T(1,128)} %bitcast.21), custom_call_target="tpu_custom_call" | custom-call | flops 100663296 | bytes 6291456 | tf_op jit(solution)/shard_map/dense/pallas_call | solution.py:230
  40.2 12.6 %all-to-all-done = bf16[64,2,2048]{2,1,0:T(2,128)(2,1)S(1)} async-done(((bf16[64,2,2048]{2,1,0:T(2,128)(2,1)}), bf16[64,2,2048]{2,1,0:T(2,128)(2,1)S(1)}, u32[]{:S(2)}, u32[]{:S(2)}) %all-to-all-start) | async-done | bytes 524320 | tf_op jit(solution)/shard_map/all_to_all | solution.py:366
  52.8 1.0 %reshape.17.rows = bf16[128,2048]{1,0:T(8,128)(2,1)} reshape(bf16[64,2,2048]{2,1,0:T(2,128)(2,1)S(1)} %all-to-all-done) | data formatting | bytes 1048576 | tf_op jit(solution)/shard_map/reshape | solution.py:371
  53.8 3.5 %experts.1 = (bf16[160,512]{1,0:T(8,128)(2,1)}, bf16[160,512]{1,0:T(8,128)(2,1)}, bf16[160,512]{1,0:T(8,128)(2,1)}, bf16[160,512]{1,0:T(8,128)(2,1)}) custom-call(s32[1]{0:T(128)} %bitcast.place, bf16[128,2048]{1,0:T(8,128)(2,1)} %reshape.17.rows, bf16[2048,256]{1,0:T(8,128)(2,1)} %bitcast.14, bf16[2048,256]{1,0:T(8,128)(2,1)} %bitcast.15, ...), custom_call_target="tpu_custom_call" | custom-call | tf_op jit(solution)/shard_map/experts/pallas_call | solution.py:263
  57.3 1.5 %collective-permute-start.4 = (bf16[160,512]{1,0:T(8,128)(2,1)}, bf16[160,512]{1,0:T(8,128)(2,1)S(1)}, u32[]{:S(2)}, u32[]{:S(2)}) collective-permute-start(bf16[160,512]{1,0:T(8,128)(2,1)} %get-tuple-element.27), channel_id=1, source_target_pairs={{0,2},{1,3},{2,0},{3,1},{4,6},{5,7},{6,4},{7,5},{8,10},{9,11},{10,... | collective-permute-start | bytes 491528 | tf_op jit(solution)/shard_map/ppermute | solution.py:325
  58.8 1.6 %collective-permute-start.5 = (bf16[160,512]{1,0:T(8,128)(2,1)}, bf16[160,512]{1,0:T(8,128)(2,1)S(1)}, u32[]{:S(2)}, u32[]{:S(2)}) collective-permute-start(bf16[160,512]{1,0:T(8,128)(2,1)} %get-tuple-element.28), channel_id=1, source_target_pairs={{0,3},{1,0},{2,1},{3,2},{4,7},{5,4},{6,5},{7,6},{8,11},{9,8},{10,9... | collective-permute-start | bytes 491528 | tf_op jit(solution)/shard_map/ppermute | solution.py:325
  60.5 7.2 %collective-permute-done.3.one = bf16[160,512]{1,0:T(8,128)(2,1)S(1)} collective-permute-done((bf16[160,512]{1,0:T(8,128)(2,1)}, bf16[160,512]{1,0:T(8,128)(2,1)S(1)}, u32[]{:S(2)}, u32[]{:S(2)}) %collective-permute-start.3) | collective-permute-done | bytes 163872 | tf_op jit(solution)/shard_map/ppermute | solution.py:325
  67.6 0.4 collective-permute-done.5.three
  68.7 2.0 %gather.1 = (bf16[128,512]{1,0:T(8,128)(2,1)}, f32[16,512]{1,0:T(8,128)}) custom-call(s32[1]{0:T(128)} %bitcast.place, bf16[160,512]{1,0:T(8,128)(2,1)} %get-tuple-element.25.own, bf16[160,512]{1,0:T(8,128)(2,1)} %copy-done, bf16[160,512]{1,0:T(8,128)(2,1)} %copy-done.1, bf16[160,512]{1,0:T(8,128)(2,1)} %copy-done.2, f32[16,2048]{1,0:T(8,128)} %get-tuple-element.29.residual), custom_call_target="tpu_custom_call" | custom-call | tf_op jit(solution)/shard_map/gather/pallas_call | solution.py:290
  70.7 1.0 %reshape.18 = bf16[64,2,512]{2,1,0:T(2,128)(2,1)S(1)} reshape(bf16[128,512]{1,0:T(8,128)(2,1)} %get-tuple-element.32) | data formatting | bytes 262144 | tf_op jit(solution)/shard_map/reshape | solution.py:377
  71.7 17.3 %all_to_all.10 = bf16[64,2,512]{2,1,0:T(2,128)(2,1)S(1)} all-to-all(bf16[64,2,512]{2,1,0:T(2,128)(2,1)S(1)} %reshape.18), channel_id=1, replica_groups=mesh['ep'=64,'tp'=4] {'ep'}, dimensions={0} | all-to-all | bytes 262144 | tf_op jit(solution)/shard_map/all_to_all | solution.py:376
  88.9 0.7 reshape.19.returned
  89.7 1.8 %combine.1 = bf16[16,512]{1,0:T(8,128)(2,1)} custom-call(f32[16,512]{1,0:T(8,128)} %get-tuple-element.30.kept, f32[128,16]{1,0:T(8,128)} %get-tuple-element.31.mix, bf16[128,512]{1,0:T(8,128)(2,1)} %reshape.19.returned), custom_call_target="tpu_custom_call" | custom-call | tf_op jit(solution)/shard_map/combine/pallas_call | solution.py:314
  (13 shorter events, 0.7 us)
Async XLA Ops:
  7.4 5.0 %collective-permute-start.2 = (bf16[16,2048]{1,0:T(8,128)(2,1)}, bf16[16,2048]{1,0:T(8,128)(2,1)S(1)}, u32[]{:S(2)}, u32[]{:S(2)}) collective-permute-start(bf16[16,2048]{1,0:T(8,128)(2,1)} %get-tuple-element.19.own), channel_id=1, source_target_pairs={{0,3},{1,0},{2,1},{3,2},{4,7},{5,4},{6,5},{7,6},{8,11},{9,8},{10,9... | collective-permute-start | bytes 196616 | tf_op jit(solution)/shard_map/ppermute | solution.py:325
  10.8 4.9 %collective-permute-start.1 = (bf16[16,2048]{1,0:T(8,128)(2,1)}, bf16[16,2048]{1,0:T(8,128)(2,1)S(1)}, u32[]{:S(2)}, u32[]{:S(2)}) collective-permute-start(bf16[16,2048]{1,0:T(8,128)(2,1)} %get-tuple-element.19.own), channel_id=1, source_target_pairs={{0,2},{1,3},{2,0},{3,1},{4,6},{5,7},{6,4},{7,5},{8,10},{9,11},{10,... | collective-permute-start | bytes 196616 | tf_op jit(solution)/shard_map/ppermute | solution.py:325
  11.3 5.0 %collective-permute-start = (bf16[16,2048]{1,0:T(8,128)(2,1)}, bf16[16,2048]{1,0:T(8,128)(2,1)S(1)}, u32[]{:S(2)}, u32[]{:S(2)}) collective-permute-start(bf16[16,2048]{1,0:T(8,128)(2,1)} %get-tuple-element.19.own), channel_id=1, source_target_pairs={{0,1},{1,2},{2,3},{3,0},{4,5},{5,6},{6,7},{7,4},{8,9},{9,10},{10,1... | collective-permute-start | bytes 196616 | tf_op jit(solution)/shard_map/ppermute | solution.py:325
  12.5 3.9 %copy-start.3 = (bf16[16,2048]{1,0:T(8,128)(2,1)}, bf16[16,2048]{1,0:T(8,128)(2,1)S(1)}, u32[]{:S(2)}) copy-start(bf16[16,2048]{1,0:T(8,128)(2,1)S(1)} %collective-permute-done.2.three) | copy-start | bytes 196612
  15.7 0.7 copy-start.4
  16.3 0.6 copy-start.5
  21.4 31.5 %all-to-all-start = ((bf16[64,2,2048]{2,1,0:T(2,128)(2,1)}), bf16[64,2,2048]{2,1,0:T(2,128)(2,1)S(1)}, u32[]{:S(2)}, u32[]{:S(2)}) async-start(bf16[64,2,2048]{2,1,0:T(2,128)(2,1)} %reshape.16), calls=%async_computation | async-start | bytes 1048576 | tf_op jit(solution)/shard_map/all_to_all | solution.py:366
  57.3 10.3 %collective-permute-start.3 = (bf16[160,512]{1,0:T(8,128)(2,1)}, bf16[160,512]{1,0:T(8,128)(2,1)S(1)}, u32[]{:S(2)}, u32[]{:S(2)}) collective-permute-start(bf16[160,512]{1,0:T(8,128)(2,1)} %get-tuple-element.26), channel_id=1, source_target_pairs={{0,1},{1,2},{2,3},{3,0},{4,5},{5,6},{6,7},{7,4},{8,9},{9,10},{10,1... | collective-permute-start | bytes 491528 | tf_op jit(solution)/shard_map/ppermute | solution.py:325
  57.3 10.3 %collective-permute-start.4 = (bf16[160,512]{1,0:T(8,128)(2,1)}, bf16[160,512]{1,0:T(8,128)(2,1)S(1)}, u32[]{:S(2)}, u32[]{:S(2)}) collective-permute-start(bf16[160,512]{1,0:T(8,128)(2,1)} %get-tuple-element.27), channel_id=1, source_target_pairs={{0,2},{1,3},{2,0},{3,1},{4,6},{5,7},{6,4},{7,5},{8,10},{9,11},{10,... | collective-permute-start | bytes 491528 | tf_op jit(solution)/shard_map/ppermute | solution.py:325
  58.8 9.2 %collective-permute-start.5 = (bf16[160,512]{1,0:T(8,128)(2,1)}, bf16[160,512]{1,0:T(8,128)(2,1)S(1)}, u32[]{:S(2)}, u32[]{:S(2)}) collective-permute-start(bf16[160,512]{1,0:T(8,128)(2,1)} %get-tuple-element.28), channel_id=1, source_target_pairs={{0,3},{1,0},{2,1},{3,2},{4,7},{5,4},{6,5},{7,6},{8,11},{9,8},{10,9... | collective-permute-start | bytes 491528 | tf_op jit(solution)/shard_map/ppermute | solution.py:325
  67.6 0.7 copy-start
  67.6 0.7 copy-start.1
  68.1 0.7 copy-start.2

commit v2 on v1

v2 whole, which is shorter than its diff:
```python
import jax
import jax.numpy as jnp
from jax import lax
from jax.experimental import pallas as pl
from jax.experimental.pallas import tpu as pltpu
from jax.sharding import PartitionSpec as P

HEADS = 8
KV_HEADS = 4
DQK = 64
DV = 128
TOPK = 4
CAP = 2
GROUP = 4

epsilon = 1e-06
F32 = jnp.float32
BF16 = jnp.bfloat16


def rms_scale(values, gain):
    return values * lax.rsqrt(jnp.mean(values * values, axis=-1, keepdims=True) + epsilon) * gain


def dot(lhs, rhs, contract=((1,), (0,))):
    return lax.dot_general(lhs, rhs, (contract, ((), ())), preferred_element_type=F32)


def attention_kernel(
    lengths_hbm,
    lambdas_hbm,
    tokens_hbm,
    norm_gain_hbm,
    head_gain_hbm,
    query_hbm,
    key_hbm,
    value_hbm,
    output_hbm,
    key_cache,
    value_cache,
    partial_out,
    lengths,
    lambdas,
    tokens,
    norm_gain,
    head_gain,
    query_weight,
    key_weight,
    value_weight,
    output_weight,
    keys,
    values,
    mixture,
    sems,
):
    seq_count = tokens.shape[0]
    groups = seq_count // GROUP
    pairs = [
        (tokens_hbm, tokens),
        (norm_gain_hbm, norm_gain),
        (query_hbm, query_weight),
        (key_hbm, key_weight),
        (value_hbm, value_weight),
        (lengths_hbm, lengths),
        (lambdas_hbm, lambdas),
        (head_gain_hbm, head_gain),
    ]
    for group in range(groups):
        rows = pl.ds(group * GROUP, GROUP)
        pairs.append((key_cache.at[rows], keys.at[rows]))
        pairs.append((value_cache.at[rows], values.at[rows]))
    pairs.append((output_hbm, output_weight))
    copies = [
        pltpu.make_async_copy(source, target, sems.at[i])
        for i, (source, target) in enumerate(pairs)
    ]
    for copy in copies:
        copy.start()
    last = copies.pop()
    copies[0].wait()
    copies[1].wait()
    normed = rms_scale(tokens[...].astype(F32), norm_gain[...]).astype(BF16)
    copies[2].wait()
    queries = dot(normed, query_weight[...]).astype(BF16).astype(F32)
    copies[3].wait()
    new_keys = dot(normed, key_weight[...]).astype(BF16).astype(F32)
    copies[4].wait()
    new_values = dot(normed, value_weight[...]).astype(BF16).astype(F32)

    for copy in copies[5:8]:
        copy.wait()
    cache_len = keys.shape[1]
    row = lax.broadcasted_iota(jnp.int32, (8, 2 * DQK), 0)
    lane = lax.broadcasted_iota(jnp.int32, (8, 2 * DQK), 1)
    keep = jnp.logical_and((lane // DQK) == (row % 2), row < 4)
    row1 = lax.broadcasted_iota(jnp.int32, (8, 1), 0)
    sign = jnp.where(row1 % 2 == 0, 1.0, -jnp.where(row1 < 2, lambdas[0], lambdas[1]))
    position = lax.broadcasted_iota(jnp.int32, (8, cache_len), 1)
    score_scale = DQK ** (-0.5)
    for group in range(groups):
        copies[8 + 2 * group].wait()
        scores = []
        own_scores = []
        for s in range(group * GROUP, (group + 1) * GROUP):
            first = jnp.broadcast_to(queries[s : s + 1, : 2 * DQK], (8, 2 * DQK))
            second = jnp.broadcast_to(queries[s : s + 1, 2 * DQK :], (8, 2 * DQK))
            query = jnp.where(keep, jnp.where(row < 2, first, second), 0.0)
            score = dot(query.astype(BF16), keys[s], ((1,), (1,))) * score_scale
            scores.append(jnp.where(position < lengths[s], score, -jnp.inf))
            own_scores.append(
                jnp.sum(query * new_keys[s : s + 1, :], axis=1, keepdims=True) * score_scale
            )
        weights = []
        own_weights = []
        for score, own in zip(scores, own_scores):
            top = jnp.maximum(jnp.max(score, axis=1, keepdims=True), own)
            grown = jnp.exp(score - top)
            own_grown = jnp.exp(own - top)
            total = jnp.sum(grown, axis=1, keepdims=True) + own_grown
            share = sign / total
            prob = grown * share
            own_prob = own_grown * share
            weights.append((prob + pltpu.roll(prob, 7, 0)).astype(BF16))
            own_weights.append((own_prob + pltpu.roll(own_prob, 7, 0)).astype(BF16).astype(F32))
        copies[9 + 2 * group].wait()
        for i in range(GROUP):
            s = group * GROUP + i
            mixed = dot(weights[i], values[s]) + own_weights[i] * new_values[s : s + 1, :]
            mixture[s : s + 1, :DV] = mixed[0:1, :]
            mixture[s : s + 1, DV:] = mixed[2:3, :]
    gain = head_gain[...]
    left = rms_scale(mixture[:, :DV], gain).astype(BF16)
    right = rms_scale(mixture[:, DV:], gain).astype(BF16)
    last.wait()
    result = dot(left, output_weight[:DV, :]) + dot(right, output_weight[DV:, :])
    partial_out[...] = result.astype(BF16)


def whole(count):
    return [pl.BlockSpec(memory_space=pltpu.VMEM)] * count


def near(value):
    return pltpu.with_memory_space_constraint(value, pltpu.VMEM)


def all_far(*values):
    return [pltpu.with_memory_space_constraint(value, pltpu.HBM) for value in values]


def all_near(*values):
    return [near(value) for value in values]


def attend(lengths, lambdas, tokens, norm_gain, head_gain, query_weight, key_weight, value_weight,
           output_weight, key_cache, value_cache):
    seq_count, width = tokens.shape
    vectors = (tokens, norm_gain, head_gain, query_weight, key_weight, value_weight, output_weight,
               key_cache, value_cache)
    return pl.pallas_call(
        attention_kernel,
        name="attend",
        compiler_params=pltpu.CompilerParams(vmem_limit_bytes=16 << 20),
        out_shape=pltpu.VMEM((seq_count, width), BF16),
        in_specs=[pl.BlockSpec(memory_space=pltpu.HBM)] * 11,
        out_specs=whole(1)[0],
        scratch_shapes=[
            pltpu.SMEM(lengths.shape, lengths.dtype),
            pltpu.SMEM(lambdas.shape, lambdas.dtype),
            *[pltpu.VMEM(value.shape, value.dtype) for value in vectors],
            pltpu.VMEM((seq_count, 2 * DV), F32),
            pltpu.SemaphoreType.DMA((9 + 2 * (seq_count // GROUP),)),
        ],
    )(*all_far(lengths, lambdas, *vectors))


def load_kernel(*refs):
    count = (len(refs) - 2) // 2
    sems = refs[-1]
    copies = [
        pltpu.make_async_copy(refs[1 + i], refs[1 + count + i], sems.at[i]) for i in range(count)
    ]
    for copy in copies:
        copy.start()
    for copy in copies:
        copy.wait()


def load(after, *values):
    size = sum(value.size * value.dtype.itemsize for value in values)
    return pl.pallas_call(
        load_kernel,
        name="load",
        compiler_params=pltpu.CompilerParams(vmem_limit_bytes=4 << 20),
        out_shape=tuple(pltpu.VMEM(value.shape, value.dtype) for value in values),
        in_specs=whole(1) + [pl.BlockSpec(memory_space=pltpu.HBM)] * len(values),
        out_specs=tuple(whole(len(values))),
        scratch_shapes=[pltpu.SemaphoreType.DMA((len(values),))],
        cost_estimate=pl.CostEstimate(
            flops=1 << 30, bytes_accessed=size, transcendentals=0
        ),
    )(near(after), *all_far(*values))


def slot_masks(routes, route_weight, slots):
    seq_count = routes.shape[1]
    slot_ids = lax.broadcasted_iota(jnp.int32, (slots, seq_count), 0)
    named = jnp.zeros((slots, seq_count), F32)
    weighed = jnp.zeros((slots, seq_count), F32)
    for k in range(TOPK):
        hit = (slot_ids // CAP) == routes[k : k + 1, :]
        named = named + jnp.where(hit, 1.0, 0.0)
        weighed = weighed + jnp.where(hit, route_weight[k : k + 1, :], 0.0)
    before = lax.broadcasted_iota(jnp.int32, (seq_count, seq_count), 0)
    after = lax.broadcasted_iota(jnp.int32, (seq_count, seq_count), 1)
    earlier = jnp.where(before < after, 1.0, 0.0).astype(BF16)
    rank = dot(named.astype(BF16), earlier)
    chosen = rank == (slot_ids % CAP).astype(F32)
    return jnp.where(chosen, named, 0.0), jnp.where(chosen, weighed, 0.0)


def plan_kernel(routes, route_weight, dispatch, mix):
    named, weighed = slot_masks(routes, route_weight, dispatch.shape[0])
    dispatch[...] = named.astype(BF16)
    mix[...] = weighed


def plan(routes, route_weight, slots):
    seq_count = routes.shape[1]
    return pl.pallas_call(
        plan_kernel,
        name="plan",
        compiler_params=pltpu.CompilerParams(vmem_limit_bytes=4 << 20),
        out_shape=(pltpu.VMEM((slots, seq_count), BF16), pltpu.VMEM((slots, seq_count), F32)),
        in_specs=whole(2),
        out_specs=tuple(whole(2)),
        cost_estimate=pl.CostEstimate(flops=1 << 28, bytes_accessed=1 << 10, transcendentals=0),
    )(*all_near(routes, route_weight))


def normalise_kernel(
    tokens, own, one, two, three, gain, dispatch, residual, ffn_in, outbound
):
    attention = (own[...].astype(F32) + one[...].astype(F32)) + (
        two[...].astype(F32) + three[...].astype(F32)
    )
    total = tokens[...].astype(F32) + attention
    residual[...] = total
    ffn_in[...] = rms_scale(total, gain[...]).astype(BF16)
    columns = outbound.shape[2]
    start = pl.multiple_of(lax.axis_index("tp") * columns, columns)
    sent = dot(dispatch[...], ffn_in[:, pl.ds(start, columns)]).astype(BF16)
    outbound[...] = sent.reshape(outbound.shape)


def normalise(tokens, parts, gain, dispatch, columns):
    seq_count, width = tokens.shape
    return pl.pallas_call(
        normalise_kernel,
        name="normalise",
        compiler_params=pltpu.CompilerParams(vmem_limit_bytes=8 << 20),
        out_shape=(
            pltpu.VMEM((seq_count, width), F32),
            pltpu.VMEM((seq_count, width), BF16),
            pltpu.VMEM((dispatch.shape[0] // CAP, CAP, columns), BF16),
        ),
        in_specs=whole(7),
        out_specs=tuple(whole(3)),
    )(*all_near(tokens, *parts, gain, dispatch))


def silu(values):
    return values / (1.0 + jnp.exp(-values))


def dense_kernel(rows, gate, up, down, vector, term, logit):
    value = rows[...]
    gate_pre = dot(value, gate[...], ((1,), (1,)))
    up_proj = dot(value, up[...], ((1,), (1,)))
    hidden = (silu(gate_pre) * up_proj).astype(BF16)
    term[...] = dot(hidden, down[...]).astype(BF16)
    part = jnp.sum(hidden.astype(F32) * vector[...], axis=1, keepdims=True)
    high = part.astype(BF16)
    rest = part - high.astype(F32)
    middle = rest.astype(BF16)
    low = (rest - middle.astype(F32)).astype(BF16)
    lane = lax.broadcasted_iota(jnp.int32, logit.shape, 1)
    pieces = jnp.where(
        lane == 0, high.astype(F32), jnp.where(lane == 1, middle.astype(F32), low.astype(F32))
    )
    logit[...] = jnp.where(lane < 3, pieces, 0.0).astype(BF16)


def dense_branch(rows, gate, up, down, vector, columns):
    seq_count, width = rows.shape
    return pl.pallas_call(
        dense_kernel,
        name="dense",
        compiler_params=pltpu.CompilerParams(vmem_limit_bytes=8 << 20),
        out_shape=(
            pltpu.VMEM((seq_count, width), BF16),
            pltpu.VMEM((seq_count, columns), BF16),
        ),
        in_specs=whole(5),
        out_specs=tuple(whole(2)),
        cost_estimate=pl.CostEstimate(
            flops=6 * seq_count * width * gate.shape[0],
            bytes_accessed=6 * width * gate.shape[0],
            transcendentals=0,
        ),
    )(*all_near(rows, gate, up, down, vector))


def expert_kernel(own, one, two, three, gate, up, down, term, logit, *blocks):
    devices = len(blocks)
    place = lax.axis_index("tp")
    count, columns = own.shape[0] * own.shape[1], own.shape[2]
    seq_count = term.shape[0]
    gate_pre = jnp.zeros((count, gate.shape[1]), F32)
    up_proj = jnp.zeros((count, up.shape[1]), F32)
    for step, part in enumerate((own, one, two, three)):
        start = pl.multiple_of(((place + devices - step) % devices) * columns, columns)
        rows = part[...].reshape(count, columns)
        gate_pre = gate_pre + dot(rows, gate[pl.ds(start, columns), :])
        up_proj = up_proj + dot(rows, up[pl.ds(start, columns), :])
    hidden = (silu(gate_pre) * up_proj).astype(BF16)
    for step, block in enumerate(blocks):
        start = pl.multiple_of(((place + step) % devices) * columns, columns)
        block[:count, :] = dot(hidden, down[:, pl.ds(start, columns)]).astype(BF16)
        block[count : count + seq_count, :] = term[:, pl.ds(start, columns)]
        block[count + seq_count :, :] = logit[...]


def expert_rows(parts, gate, up, down, term, logit):
    devices = len(parts)
    experts, cap, columns = parts[0].shape
    shape = pltpu.VMEM((experts * cap + 2 * term.shape[0], columns), BF16)
    return pl.pallas_call(
        expert_kernel,
        name="experts",
        compiler_params=pltpu.CompilerParams(vmem_limit_bytes=8 << 20),
        out_shape=(shape,) * devices,
        in_specs=whole(9),
        out_specs=tuple(whole(devices)),
    )(*all_near(*parts, gate, up, down, term, logit))


def gather_kernel(own, one, two, three, residual, summed, kept):
    count, columns = summed.shape[0] * summed.shape[1], summed.shape[2]
    seq_count = residual.shape[0]
    total = (own[...].astype(F32) + one[...].astype(F32)) + (
        two[...].astype(F32) + three[...].astype(F32)
    )
    summed[...] = total[:count, :].astype(BF16).reshape(summed.shape)
    pieces = total[count + seq_count :, :]
    lane = lax.broadcasted_iota(jnp.int32, pieces.shape, 1)
    logit = jnp.sum(jnp.where(lane < 3, pieces, 0.0), axis=1, keepdims=True)
    gated = total[count : count + seq_count, :] / (1.0 + jnp.exp(-logit))
    start = pl.multiple_of(lax.axis_index("tp") * columns, columns)
    kept[...] = residual[:, pl.ds(start, columns)] + gated


def gather_parts(parts, residual, count):
    seq_count = residual.shape[0]
    columns = parts[0].shape[1]
    return pl.pallas_call(
        gather_kernel,
        name="gather",
        compiler_params=pltpu.CompilerParams(vmem_limit_bytes=8 << 20),
        out_shape=(
            pltpu.VMEM((count // CAP, CAP, columns), BF16),
            pltpu.VMEM((seq_count, columns), F32),
        ),
        in_specs=whole(5),
        out_specs=tuple(whole(2)),
    )(*all_near(*parts, residual))


def combine_kernel(kept, mix, returned, out):
    picked = lax.dot_general(
        mix[...],
        returned[...].reshape(mix.shape[0], -1).astype(F32),
        (((0,), (0,)), ((), ())),
        precision=lax.Precision.HIGHEST,
        preferred_element_type=F32,
    )
    out[...] = (kept[...] + picked).astype(BF16)


def combine(kept, mix, returned):
    return pl.pallas_call(
        combine_kernel,
        name="combine",
        compiler_params=pltpu.CompilerParams(vmem_limit_bytes=8 << 20),
        out_shape=jax.ShapeDtypeStruct(kept.shape, BF16),
        in_specs=whole(3),
        out_specs=whole(1)[0],
    )(*all_near(kept, mix, returned))


def passed_on(shard, step):
    devices = lax.axis_size("tp")
    return lax.ppermute(shard, "tp", [(i, (i + step) % devices) for i in range(devices)])


def shards(
    tokens,
    norm_gain,
    query_weight,
    key_weight,
    value_weight,
    output_weight,
    head_gain,
    lambdas,
    key_cache,
    value_cache,
    lengths,
    ffn_gain,
    routes,
    route_weight,
    expert_gate,
    expert_up,
    expert_down,
    dense_gate,
    dense_up,
    dense_down,
    gate_vector,
):
    seq_count, width = tokens.shape
    cache_len = key_cache.shape[1]
    devices = lax.axis_size("tp")
    experts_total = lax.axis_size("ep")
    slots = experts_total * CAP
    columns = width // devices
    keys = jnp.transpose(key_cache, (0, 2, 1, 3)).reshape(seq_count, cache_len, 2 * DQK)
    values = jnp.transpose(value_cache, (0, 2, 1, 3)).reshape(seq_count, cache_len, DV)
    partial = attend(
        lengths, lambdas, tokens, norm_gain[None], head_gain[None], query_weight, key_weight,
        value_weight, output_weight, keys, values,
    )
    parts = [partial] + [passed_on(partial, step) for step in range(1, devices)]
    (
        route_rows, weight_rows, near_tokens, near_gain, near_gate_vector,
        near_dense_gate, near_dense_up, near_dense_down,
        near_expert_gate, near_expert_up, near_expert_down,
    ) = load(
        partial, routes.T, route_weight.T, tokens, ffn_gain[None], gate_vector[None],
        dense_gate, dense_up, dense_down, expert_gate[0], expert_up[0], expert_down[0],
    )
    dispatch, mix = plan(route_rows, weight_rows, slots)
    residual, ffn_in, outbound = normalise(
        near_tokens, parts, near_gain, dispatch, columns
    )
    arrived = lax.all_to_all(outbound, "ep", split_axis=0, concat_axis=0, tiled=True)
    arrived, ffn_in = lax.optimization_barrier((arrived, ffn_in))
    term, logit = dense_branch(
        ffn_in, near_dense_gate, near_dense_up, near_dense_down, near_gate_vector, columns
    )
    gathered = [arrived] + [passed_on(arrived, step) for step in range(1, devices)]
    blocks = expert_rows(
        gathered, near_expert_gate, near_expert_up, near_expert_down, term, logit
    )
    moved = [blocks[0]] + [passed_on(blocks[step], step) for step in range(1, devices)]
    summed, kept = gather_parts(moved, residual, slots)
    returned = lax.all_to_all(summed, "ep", split_axis=0, concat_axis=0, tiled=True)
    return combine(kept, mix, returned)


def solution(mesh):
    placed = (
        P("ep", None),
        P(),
        P(None, "tp"),
        P(None, "tp"),
        P(None, "tp"),
        P("tp", None),
        P(),
        P("tp"),
        P("ep", None, "tp", None),
        P("ep", None, "tp", None),
        P("ep"),
        P(),
        P("ep", None),
        P("ep", None),
        P("ep", None, "tp"),
        P("ep", None, "tp"),
        P("ep", "tp", None),
        P("tp", None),
        P("tp", None),
        P("tp", None),
        P("tp"),
    )
    return jax.shard_map(
        shards, mesh=mesh, in_specs=placed, out_specs=P("ep", "tp"), check_vma=False
    )
```

time: 91.9 us -> 79 us (0.86)
  blocking collectives: 17.3 us -> 40.6 us
  waiting for transfers between devices: 24.6 us -> 13.7 us
  starting transfers between devices: 21.4 us -> 10.7 us
  Pallas kernels: 22 us -> 13.7 us
  local copies, waits for them, and re-layouts: 6.17 us -> 0 us
    all_to_all x1 -> x2, blocking collectives: 17.3 us -> 40.6 us  [the longest x1 24.6 us: shards(): lax.all_to_all(outbound, 'ep', split_axis=0, concat_axis=0, tiled=True)]
    all_to_all x1 -> x0, starting transfers between devices: 13.8 us -> none  [shards(): lax.all_to_all(outbound.reshape(experts_total, CAP, width), 'ep', split_a...]
    all_to_all x1 -> x0, waiting for transfers between devices: 12.6 us -> none  [shards(): lax.all_to_all(outbound.reshape(experts_total, CAP, width), 'ep', split_a...]
    pallas_call x6 -> x8, Pallas kernels: 22 us -> 13.7 us  [the longest x1 6.04 us: attend(): pl.pallas_call(attention_kernel, name='attend', compiler_params=pltpu.Com...]
    reshape x4 -> x0, local copies, waits for them, and re-layouts: 4.87 us -> none  [the longest x1 2.18 us: shards(): outbound.reshape(experts_total, CAP, width)]
    ppermute x6 -> x9, starting transfers between devices: 7.62 us -> 10.7 us  [passed_on(): lax.ppermute(shard, 'tp', [(i, (i + step) % devices) for i in range(devic...]
    ppermute x6 -> x9, waiting for transfers between devices: 12 us -> 13.7 us  [passed_on(): lax.ppermute(shard, 'tp', [(i, (i + step) % devices) for i in range(devic...]
    unnamed x12 -> x0, local copies, waits for them, and re-layouts: 1.3 us -> none
  transfers between devices with their start and end apart: 7 -> 9, of which waited for: 6 -> 7; matrix products, arithmetic and copies ran while one was open for 0% -> 0% of each run, Pallas kernels for 6% -> 7%
where the time goes in v2:
time: 79 us; the launch traced here: 78.8 us
  blocking collectives  40.6 us (51%)
  Pallas kernels  13.7 us (17%)
  waiting for transfers between devices  13.7 us (17%)
  starting transfers between devices  10.7 us (14%)
    all_to_all x1, blocking collectives, shards(): lax.all_to_all(outbound, 'ep', split_axis=0, concat_axis=0, tiled=True)  24.6 us
    all_to_all x1, blocking collectives, shards(): lax.all_to_all(summed, 'ep', split_axis=0, concat_axis=0, tiled=True)  16 us
    ppermute x9, waiting for transfers between devices, passed_on(): lax.ppermute(shard, 'tp', [(i, (i + step) % devices) for i in range(devic...  13.7 us
    ppermute x9, starting transfers between devices, passed_on(): lax.ppermute(shard, 'tp', [(i, (i + step) % devices) for i in range(devic...  10.7 us
    pallas_call x1, Pallas kernels, attend(): pl.pallas_call(attention_kernel, name='attend', compiler_params=pltpu.Com...  6.04 us
    pallas_call x1, Pallas kernels, load(): pl.pallas_call(load_kernel, name='load', compiler_params=pltpu.CompilerPa...  3.88 us
  transfers between devices with their start and end apart: 9, of which 7 were waited for; matrix products, arithmetic and copies ran while one was open for 0% of the time, Pallas kernels for 7%

profile of v2, /device:TPU:1, one launch (start us, length us, event | category | flops | bytes accessed | tf_op | source)
XLA Modules:
  0.0 78.8 jit_solution(919188682004650518)
XLA Ops:
  0.0 6.0 %attend.1.refs_0_.own = bf16[16,2048]{1,0:T(8,128)(2,1)S(1)} custom-call(s32[16]{0:T(128)} %lengths_hbm.1, f32[2]{0:T(128)} %lambdas_hbm.1, bf16[16,2048]{1,0:T(8,128)(2,1)} %refs_3_.1, f32[1,2048]{1,0:T(1,128)} %bitcast.16, f32[1,128]{1,0:T(1,128)} %bitcast.21, bf16[2048,256]{1,0:T(8,128)(2,1)} %query_hbm.1, bf16[2048,128]{1,0:T(8,128)(2,1)} %key_hbm.1, ...), custom_call_target="tpu_custom_call" | custom-call | tf_op jit(solution)/shard_map/attend/pallas_call | solution.py:160
  6.0 3.4 %collective-permute-start.2 = (bf16[16,2048]{1,0:T(8,128)(2,1)S(1)}, bf16[16,2048]{1,0:T(8,128)(2,1)S(1)}, u32[]{:S(2)}, u32[]{:S(2)}) collective-permute-start(bf16[16,2048]{1,0:T(8,128)(2,1)S(1)} %attend.1.refs_0_.own), channel_id=1, source_target_pairs={{0,3},{1,0},{2,1},{3,2},{4,7},{5,4},{6,5},{7,6},{8,11},{9,8},{10,9... | collective-permute-start | bytes 196616 | tf_op jit(solution)/shard_map/ppermute | solution.py:403
  9.4 0.5 collective-permute-start.1
  9.9 0.6 collective-permute-start
  10.5 3.9 %load.1 = (s32[4,16]{1,0:T(4,128)S(1)}, f32[4,16]{1,0:T(4,128)S(1)}, bf16[16,2048]{1,0:T(8,128)(2,1)S(1)}, f32[1,2048]{1,0:T(1,128)S(1)}, f32[1,512]{1,0:T(1,128...) custom-call(bf16[16,2048]{1,0:T(8,128)(2,1)S(1)} %attend.1.refs_0_.o, ...), custom_call_target="tpu_custom_call" | custom-call | flops 1073741824 | bytes 9513472 | tf_op jit(solution)/shard_map/load/pallas_call | solution.py:191
  14.4 0.2 plan.1
  14.6 0.1 collective-permute-done.one
  14.7 0.3 normalise.1
  15.1 24.6 %all_to_all.10.own = bf16[64,2,512]{2,1,0:T(2,128)(2,1)S(1)} all-to-all(bf16[64,2,512]{2,1,0:T(2,128)(2,1)S(1)} %get-tuple-element.36), channel_id=1, replica_groups=mesh['ep'=64,'tp'=4] {'ep'}, dimensions={0} | all-to-all | bytes 262144 | tf_op jit(solution)/shard_map/all_to_all | solution.py:454
  39.7 1.4 %collective-permute-start.5 = (bf16[64,2,512]{2,1,0:T(2,128)(2,1)S(1)}, bf16[64,2,512]{2,1,0:T(2,128)(2,1)S(1)}, u32[]{:S(2)}, u32[]{:S(2)}) collective-permute-start(bf16[64,2,512]{2,1,0:T(2,128)(2,1)S(1)} %all_to_all.10.own), channel_id=1, source_target_pairs={{0,3},{1,0},{2,1},{3,2},{4,7},{5,4},{6,5},{7,6},{8,11},{9,8},{10,9... | collective-permute-start | bytes 393224 | tf_op jit(solution)/shard_map/ppermute | solution.py:403
  41.1 1.2 %collective-permute-start.4 = (bf16[64,2,512]{2,1,0:T(2,128)(2,1)S(1)}, bf16[64,2,512]{2,1,0:T(2,128)(2,1)S(1)}, u32[]{:S(2)}, u32[]{:S(2)}) collective-permute-start(bf16[64,2,512]{2,1,0:T(2,128)(2,1)S(1)} %all_to_all.10.own), channel_id=1, source_target_pairs={{0,2},{1,3},{2,0},{3,1},{4,6},{5,7},{6,4},{7,5},{8,10},{9,11},{10,... | collective-permute-start | bytes 393224 | tf_op jit(solution)/shard_map/ppermute | solution.py:403
  42.3 1.5 %dense.1 = (bf16[16,2048]{1,0:T(8,128)(2,1)S(1)}, bf16[16,512]{1,0:T(8,128)(2,1)S(1)}) custom-call(bf16[16,2048]{1,0:T(8,128)(2,1)S(1)} %get-tuple-element.42.rows, bf16[512,2048]{1,0:T(8,128)(2,1)S(1)} %get-tuple-element.43.gate, bf16[512,2048]{1,0:T(8,128)(2,1)S(1)} %get-tuple-element.44.up, bf16[512,2048]{1,0:T(8,128)(2,1)S(1)} %get-tuple-element.45.down, ...), custom_call_target="tpu_custom_call" | custom-call | flops 100663296 | bytes 6291456 | tf_op jit(solution)/shard_map/dense/pallas_call | solution.py:296
  43.9 0.5 collective-permute-done.5.three
  44.4 2.6 %collective-permute-done.4.two = bf16[64,2,512]{2,1,0:T(2,128)(2,1)S(1)} collective-permute-done((bf16[64,2,512]{2,1,0:T(2,128)(2,1)S(1)}, bf16[64,2,512]{2,1,0:T(2,128)(2,1)S(1)}, u32[]{:S(2)}, u32[]{:S(2)}) %collective-permute-start.4) | collective-permute-done | bytes 131104 | tf_op jit(solution)/shard_map/ppermute | solution.py:403
  47.0 3.6 %collective-permute-done.3.one = bf16[64,2,512]{2,1,0:T(2,128)(2,1)S(1)} collective-permute-done((bf16[64,2,512]{2,1,0:T(2,128)(2,1)S(1)}, bf16[64,2,512]{2,1,0:T(2,128)(2,1)S(1)}, u32[]{:S(2)}, u32[]{:S(2)}) %collective-permute-start.3) | collective-permute-done | bytes 131104 | tf_op jit(solution)/shard_map/ppermute | solution.py:403
  50.6 0.8 experts.1
  51.4 1.6 %collective-permute-start.7 = (bf16[160,512]{1,0:T(8,128)(2,1)S(1)}, bf16[160,512]{1,0:T(8,128)(2,1)S(1)}, u32[]{:S(2)}, u32[]{:S(2)}) collective-permute-start(bf16[160,512]{1,0:T(8,128)(2,1)S(1)} %get-tuple-element.51), channel_id=1, source_target_pairs={{0,2},{1,3},{2,0},{3,1},{4,6},{5,7},{6,4},{7,5},{8,10},{9,11},{10,... | collective-permute-start | bytes 491528 | tf_op jit(solution)/shard_map/ppermute | solution.py:403
  53.0 2.0 %collective-permute-start.8 = (bf16[160,512]{1,0:T(8,128)(2,1)S(1)}, bf16[160,512]{1,0:T(8,128)(2,1)S(1)}, u32[]{:S(2)}, u32[]{:S(2)}) collective-permute-start(bf16[160,512]{1,0:T(8,128)(2,1)S(1)} %get-tuple-element.52), channel_id=1, source_target_pairs={{0,3},{1,0},{2,1},{3,2},{4,7},{5,4},{6,5},{7,6},{8,11},{9,8},{10,9... | collective-permute-start | bytes 491528 | tf_op jit(solution)/shard_map/ppermute | solution.py:403
  55.0 3.9 %collective-permute-done.6.one = bf16[160,512]{1,0:T(8,128)(2,1)S(1)} collective-permute-done((bf16[160,512]{1,0:T(8,128)(2,1)S(1)}, bf16[160,512]{1,0:T(8,128)(2,1)S(1)}, u32[]{:S(2)}, u32[]{:S(2)}) %collective-permute-start.6) | collective-permute-done | bytes 163872 | tf_op jit(solution)/shard_map/ppermute | solution.py:403
  58.9 1.1 %collective-permute-done.7.two = bf16[160,512]{1,0:T(8,128)(2,1)S(1)} collective-permute-done((bf16[160,512]{1,0:T(8,128)(2,1)S(1)}, bf16[160,512]{1,0:T(8,128)(2,1)S(1)}, u32[]{:S(2)}, u32[]{:S(2)}) %collective-permute-start.7) | collective-permute-done | bytes 163872 | tf_op jit(solution)/shard_map/ppermute | solution.py:403
  60.0 1.8 %collective-permute-done.8.three = bf16[160,512]{1,0:T(8,128)(2,1)S(1)} collective-permute-done((bf16[160,512]{1,0:T(8,128)(2,1)S(1)}, bf16[160,512]{1,0:T(8,128)(2,1)S(1)}, u32[]{:S(2)}, u32[]{:S(2)}) %collective-permute-start.8) | collective-permute-done | bytes 163872 | tf_op jit(solution)/shard_map/ppermute | solution.py:403
  61.8 0.1 gather.1
  61.9 16.0 %all_to_all.11.returned = bf16[64,2,512]{2,1,0:T(2,128)(2,1)S(1)} all-to-all(bf16[64,2,512]{2,1,0:T(2,128)(2,1)S(1)} %get-tuple-element.56), channel_id=1, replica_groups=mesh['ep'=64,'tp'=4] {'ep'}, dimensions={0} | all-to-all | bytes 262144 | tf_op jit(solution)/shard_map/all_to_all | solution.py:465
  77.9 0.9 %combine.1 = bf16[16,512]{1,0:T(8,128)(2,1)} custom-call(f32[16,512]{1,0:T(8,128)S(1)} %get-tuple-element.54.kept, f32[128,16]{1,0:T(8,128)S(1)} %get-tuple-element.55.mix, bf16[64,2,512]{2,1,0:T(2,128)(2,1)S(1)} %all_to_all.11.returned), custom_call_target="tpu_custom_call" | custom-call | tf_op jit(solution)/shard_map/combine/pallas_call | solution.py:391
  (4 shorter events, 0.1 us)
Async XLA Ops:
  6.0 8.6 %collective-permute-start.2 = (bf16[16,2048]{1,0:T(8,128)(2,1)S(1)}, bf16[16,2048]{1,0:T(8,128)(2,1)S(1)}, u32[]{:S(2)}, u32[]{:S(2)}) collective-permute-start(bf16[16,2048]{1,0:T(8,128)(2,1)S(1)} %attend.1.refs_0_.own), channel_id=1, source_target_pairs={{0,3},{1,0},{2,1},{3,2},{4,7},{5,4},{6,5},{7,6},{8,11},{9,8},{10,9... | collective-permute-start | bytes 196616 | tf_op jit(solution)/shard_map/ppermute | solution.py:403
  9.4 5.2 %collective-permute-start.1 = (bf16[16,2048]{1,0:T(8,128)(2,1)S(1)}, bf16[16,2048]{1,0:T(8,128)(2,1)S(1)}, u32[]{:S(2)}, u32[]{:S(2)}) collective-permute-start(bf16[16,2048]{1,0:T(8,128)(2,1)S(1)} %attend.1.refs_0_.own), channel_id=1, source_target_pairs={{0,2},{1,3},{2,0},{3,1},{4,6},{5,7},{6,4},{7,5},{8,10},{9,11},{10,... | collective-permute-start | bytes 196616 | tf_op jit(solution)/shard_map/ppermute | solution.py:403
  9.9 4.8 %collective-permute-start = (bf16[16,2048]{1,0:T(8,128)(2,1)S(1)}, bf16[16,2048]{1,0:T(8,128)(2,1)S(1)}, u32[]{:S(2)}, u32[]{:S(2)}) collective-permute-start(bf16[16,2048]{1,0:T(8,128)(2,1)S(1)} %attend.1.refs_0_.own), channel_id=1, source_target_pairs={{0,1},{1,2},{2,3},{3,0},{4,5},{5,6},{6,7},{7,4},{8,9},{9,10},{10,1... | collective-permute-start | bytes 196616 | tf_op jit(solution)/shard_map/ppermute | solution.py:403
  39.7 4.7 %collective-permute-start.5 = (bf16[64,2,512]{2,1,0:T(2,128)(2,1)S(1)}, bf16[64,2,512]{2,1,0:T(2,128)(2,1)S(1)}, u32[]{:S(2)}, u32[]{:S(2)}) collective-permute-start(bf16[64,2,512]{2,1,0:T(2,128)(2,1)S(1)} %all_to_all.10.own), channel_id=1, source_target_pairs={{0,3},{1,0},{2,1},{3,2},{4,7},{5,4},{6,5},{7,6},{8,11},{9,8},{10,9... | collective-permute-start | bytes 393224 | tf_op jit(solution)/shard_map/ppermute | solution.py:403
  41.1 5.9 %collective-permute-start.4 = (bf16[64,2,512]{2,1,0:T(2,128)(2,1)S(1)}, bf16[64,2,512]{2,1,0:T(2,128)(2,1)S(1)}, u32[]{:S(2)}, u32[]{:S(2)}) collective-permute-start(bf16[64,2,512]{2,1,0:T(2,128)(2,1)S(1)} %all_to_all.10.own), channel_id=1, source_target_pairs={{0,2},{1,3},{2,0},{3,1},{4,6},{5,7},{6,4},{7,5},{8,10},{9,11},{10,... | collective-permute-start | bytes 393224 | tf_op jit(solution)/shard_map/ppermute | solution.py:403
  42.3 8.3 %collective-permute-start.3 = (bf16[64,2,512]{2,1,0:T(2,128)(2,1)S(1)}, bf16[64,2,512]{2,1,0:T(2,128)(2,1)S(1)}, u32[]{:S(2)}, u32[]{:S(2)}) collective-permute-start(bf16[64,2,512]{2,1,0:T(2,128)(2,1)S(1)} %all_to_all.10.own), channel_id=1, source_target_pairs={{0,1},{1,2},{2,3},{3,0},{4,5},{5,6},{6,7},{7,4},{8,9},{9,10},{10,1... | collective-permute-start | bytes 393224 | tf_op jit(solution)/shard_map/ppermute | solution.py:403
  51.3 7.6 %collective-permute-start.6 = (bf16[160,512]{1,0:T(8,128)(2,1)S(1)}, bf16[160,512]{1,0:T(8,128)(2,1)S(1)}, u32[]{:S(2)}, u32[]{:S(2)}) collective-permute-start(bf16[160,512]{1,0:T(8,128)(2,1)S(1)} %get-tuple-element.50), channel_id=1, source_target_pairs={{0,1},{1,2},{2,3},{3,0},{4,5},{5,6},{6,7},{7,4},{8,9},{9,10},{10,1... | collective-permute-start | bytes 491528 | tf_op jit(solution)/shard_map/ppermute | solution.py:403
  51.4 8.6 %collective-permute-start.7 = (bf16[160,512]{1,0:T(8,128)(2,1)S(1)}, bf16[160,512]{1,0:T(8,128)(2,1)S(1)}, u32[]{:S(2)}, u32[]{:S(2)}) collective-permute-start(bf16[160,512]{1,0:T(8,128)(2,1)S(1)} %get-tuple-element.51), channel_id=1, source_target_pairs={{0,2},{1,3},{2,0},{3,1},{4,6},{5,7},{6,4},{7,5},{8,10},{9,11},{10,... | collective-permute-start | bytes 491528 | tf_op jit(solution)/shard_map/ppermute | solution.py:403
  53.0 8.8 %collective-permute-start.8 = (bf16[160,512]{1,0:T(8,128)(2,1)S(1)}, bf16[160,512]{1,0:T(8,128)(2,1)S(1)}, u32[]{:S(2)}, u32[]{:S(2)}) collective-permute-start(bf16[160,512]{1,0:T(8,128)(2,1)S(1)} %get-tuple-element.52), channel_id=1, source_target_pairs={{0,3},{1,0},{2,1},{3,2},{4,7},{5,4},{6,5},{7,6},{8,11},{9,8},{10,9... | collective-permute-start | bytes 491528 | tf_op jit(solution)/shard_map/ppermute | solution.py:403

commit v3 on v2

--- a/solution.py
+++ b/solution.py
@@ -5,8 +5,7 @@
 from jax.experimental.pallas import tpu as pltpu
 from jax.sharding import PartitionSpec as P
 
-HEADS = 8
-KV_HEADS = 4
+
 DQK = 64
 DV = 128
 TOPK = 4
@@ -273,49 +272,64 @@
     return values / (1.0 + jnp.exp(-values))
 
 
-def dense_kernel(rows, gate, up, down, vector, term, logit):
+def dense_kernel(rows, gate, up, down, vector, *refs):
+    far, near_refs, blocks, sems = refs[:3], refs[3:6], refs[6:-1], refs[-1]
+    copies = [
+        pltpu.make_async_copy(source, target, sems.at[i])
+        for i, (source, target) in enumerate(zip(far, near_refs))
+    ]
+    for copy in copies:
+        copy.start()
+    devices = len(blocks)
+    seq_count, columns = rows.shape[0], blocks[0].shape[1]
+    place = lax.axis_index("tp")
     value = rows[...]
     gate_pre = dot(value, gate[...], ((1,), (1,)))
     up_proj = dot(value, up[...], ((1,), (1,)))
     hidden = (silu(gate_pre) * up_proj).astype(BF16)
-    term[...] = dot(hidden, down[...]).astype(BF16)
     part = jnp.sum(hidden.astype(F32) * vector[...], axis=1, keepdims=True)
     high = part.astype(BF16)
     rest = part - high.astype(F32)
     middle = rest.astype(BF16)
     low = (rest - middle.astype(F32)).astype(BF16)
-    lane = lax.broadcasted_iota(jnp.int32, logit.shape, 1)
+    lane = lax.broadcasted_iota(jnp.int32, (seq_count, columns), 1)
     pieces = jnp.where(
         lane == 0, high.astype(F32), jnp.where(lane == 1, middle.astype(F32), low.astype(F32))
     )
-    logit[...] = jnp.where(lane < 3, pieces, 0.0).astype(BF16)
-
-
-def dense_branch(rows, gate, up, down, vector, columns):
+    logit = jnp.where(lane < 3, pieces, 0.0).astype(BF16)
+    for step, block in enumerate(blocks):
+        start = pl.multiple_of(((place + step) % devices) * columns, columns)
+        block[:seq_count, :] = dot(hidden, down[:, pl.ds(start, columns)]).astype(BF16)
+        block[seq_count:, :] = logit
+    for copy in copies:
+        copy.wait()
+
+
+def dense_branch(rows, gate, up, down, vector, expert_weights, devices):
     seq_count, width = rows.shape
-    return pl.pallas_call(
+    block = pltpu.VMEM((2 * seq_count, width // devices), BF16)
+    outs = pl.pallas_call(
         dense_kernel,
         name="dense",
         compiler_params=pltpu.CompilerParams(vmem_limit_bytes=8 << 20),
-        out_shape=(
-            pltpu.VMEM((seq_count, width), BF16),
-            pltpu.VMEM((seq_count, columns), BF16),
-        ),
-        in_specs=whole(5),
-        out_specs=tuple(whole(2)),
+        out_shape=tuple(pltpu.VMEM(value.shape, value.dtype) for value in expert_weights)
+        + (block,) * devices,
+        in_specs=whole(5) + [pl.BlockSpec(memory_space=pltpu.HBM)] * 3,
+        out_specs=tuple(whole(3 + devices)),
+        scratch_shapes=[pltpu.SemaphoreType.DMA((3,))],
         cost_estimate=pl.CostEstimate(
             flops=6 * seq_count * width * gate.shape[0],
             bytes_accessed=6 * width * gate.shape[0],
             transcendentals=0,
         ),
-    )(*all_near(rows, gate, up, down, vector))
-
-
-def expert_kernel(own, one, two, three, gate, up, down, term, logit, *blocks):
+    )(*all_near(rows, gate, up, down, vector), *all_far(*expert_weights))
+    return outs[:3], outs[3:]
+
+
+def expert_kernel(own, one, two, three, gate, up, down, *blocks):
     devices = len(blocks)
     place = lax.axis_index("tp")
     count, columns = own.shape[0] * own.shape[1], own.shape[2]
-    seq_count = term.shape[0]
     gate_pre = jnp.zeros((count, gate.shape[1]), F32)
     up_proj = jnp.zeros((count, up.shape[1]), F32)
     for step, part in enumerate((own, one, two, three)):
@@ -326,41 +340,42 @@
     hidden = (silu(gate_pre) * up_proj).astype(BF16)
     for step, block in enumerate(blocks):
         start = pl.multiple_of(((place + step) % devices) * columns, columns)
-        block[:count, :] = dot(hidden, down[:, pl.ds(start, columns)]).astype(BF16)
-        block[count : count + seq_count, :] = term[:, pl.ds(start, columns)]
-        block[count + seq_count :, :] = logit[...]
-
-
-def expert_rows(parts, gate, up, down, term, logit):
+        block[...] = dot(hidden, down[:, pl.ds(start, columns)]).astype(BF16)
+
+
+def expert_rows(parts, gate, up, down):
     devices = len(parts)
     experts, cap, columns = parts[0].shape
-    shape = pltpu.VMEM((experts * cap + 2 * term.shape[0], columns), BF16)
     return pl.pallas_call(
         expert_kernel,
         name="experts",
         compiler_params=pltpu.CompilerParams(vmem_limit_bytes=8 << 20),
-        out_shape=(shape,) * devices,
-        in_specs=whole(9),
+        out_shape=(pltpu.VMEM((experts * cap, columns), BF16),) * devices,
+        in_specs=whole(7),
         out_specs=tuple(whole(devices)),
-    )(*all_near(*parts, gate, up, down, term, logit))
-
-
-def gather_kernel(own, one, two, three, residual, summed, kept):
-    count, columns = summed.shape[0] * summed.shape[1], summed.shape[2]
+    )(*all_near(*parts, gate, up, down))
+
+
+def gather_kernel(own, one, two, three, dense_own, dense_one, dense_two, dense_three, residual,
+                  summed, kept):
+    columns = summed.shape[2]
     seq_count = residual.shape[0]
     total = (own[...].astype(F32) + one[...].astype(F32)) + (
         two[...].astype(F32) + three[...].astype(F32)
     )
-    summed[...] = total[:count, :].astype(BF16).reshape(summed.shape)
-    pieces = total[count + seq_count :, :]
+    summed[...] = total.astype(BF16).reshape(summed.shape)
+    dense = (dense_own[...].astype(F32) + dense_one[...].astype(F32)) + (
+        dense_two[...].astype(F32) + dense_three[...].astype(F32)
+    )
+    pieces = dense[seq_count:, :]
     lane = lax.broadcasted_iota(jnp.int32, pieces.shape, 1)
     logit = jnp.sum(jnp.where(lane < 3, pieces, 0.0), axis=1, keepdims=True)
-    gated = total[count : count + seq_count, :] / (1.0 + jnp.exp(-logit))
+    gated = dense[:seq_count, :] / (1.0 + jnp.exp(-logit))
     start = pl.multiple_of(lax.axis_index("tp") * columns, columns)
     kept[...] = residual[:, pl.ds(start, columns)] + gated
 
 
-def gather_parts(parts, residual, count):
+def gather_parts(parts, dense_parts, residual, count):
     seq_count = residual.shape[0]
     columns = parts[0].shape[1]
     return pl.pallas_call(
@@ -371,9 +386,9 @@
             pltpu.VMEM((count // CAP, CAP, columns), BF16),
             pltpu.VMEM((seq_count, columns), F32),
         ),
-        in_specs=whole(5),
+        in_specs=whole(9),
         out_specs=tuple(whole(2)),
-    )(*all_near(*parts, residual))
+    )(*all_near(*parts, *dense_parts, residual))
 
 
 def combine_kernel(kept, mix, returned, out):
@@ -442,10 +457,9 @@
     (
         route_rows, weight_rows, near_tokens, near_gain, near_gate_vector,
         near_dense_gate, near_dense_up, near_dense_down,
-        near_expert_gate, near_expert_up, near_expert_down,
     ) = load(
         partial, routes.T, route_weight.T, tokens, ffn_gain[None], gate_vector[None],
-        dense_gate, dense_up, dense_down, expert_gate[0], expert_up[0], expert_down[0],
+        dense_gate, dense_up, dense_down,
     )
     dispatch, mix = plan(route_rows, weight_rows, slots)
     residual, ffn_in, outbound = normalise(
@@ -453,15 +467,17 @@
     )
     arrived = lax.all_to_all(outbound, "ep", split_axis=0, concat_axis=0, tiled=True)
     arrived, ffn_in = lax.optimization_barrier((arrived, ffn_in))
-    term, logit = dense_branch(
-        ffn_in, near_dense_gate, near_dense_up, near_dense_down, near_gate_vector, columns
-    )
     gathered = [arrived] + [passed_on(arrived, step) for step in range(1, devices)]
-    blocks = expert_rows(
-        gathered, near_expert_gate, near_expert_up, near_expert_down, term, logit
-    )
+    expert_weights, dense_blocks = dense_branch(
+        ffn_in, near_dense_gate, near_dense_up, near_dense_down, near_gate_vector,
+        (expert_gate[0], expert_up[0], expert_down[0]), devices,
+    )
+    dense_moved = [dense_blocks[0]]
+    for step in range(1, devices):
+        dense_moved.append(passed_on(dense_blocks[step], step))
+    blocks = expert_rows(gathered, *expert_weights)
     moved = [blocks[0]] + [passed_on(blocks[step], step) for step in range(1, devices)]
-    summed, kept = gather_parts(moved, residual, slots)
+    summed, kept = gather_parts(moved, dense_moved, residual, slots)
     returned = lax.all_to_all(summed, "ep", split_axis=0, concat_axis=0, tiled=True)
     return combine(kept, mix, returned)
 
@@ -490,6 +506,7 @@
         P("tp", None),
         P("tp"),
     )
+
     return jax.shard_map(
         shards, mesh=mesh, in_specs=placed, out_specs=P("ep", "tp"), check_vma=False
     )

time: 79 us -> 81.4 us (1.030)
  blocking collectives: 40.6 us -> 41.5 us
    pallas_call x1, Pallas kernels: 1.55 us -> 3.13 us  [dense_branch(): pl.pallas_call(dense_kernel, name='dense', compiler_params=pltpu.Compiler...]
    pallas_call x1, Pallas kernels: 3.88 us -> 3.02 us  [load(): pl.pallas_call(load_kernel, name='load', compiler_params=pltpu.CompilerPa...]
    all_to_all x1, blocking collectives: 16 us -> 16.8 us  [shards(): lax.all_to_all(summed, 'ep', split_axis=0, concat_axis=0, tiled=True)]
    ppermute x9 -> x12, starting transfers between devices: 10.7 us -> 11.5 us  [passed_on(): lax.ppermute(shard, 'tp', [(i, (i + step) % devices) for i in range(devic...]
    ppermute x9 -> x12, waiting for transfers between devices: 13.7 us -> 13.8 us  [passed_on(): lax.ppermute(shard, 'tp', [(i, (i + step) % devices) for i in range(devic...]
  transfers between devices with their start and end apart: 9 -> 12, of which waited for: 7 -> 6; matrix products, arithmetic and copies ran while one was open for 0% -> 0% of each run, Pallas kernels for 7% -> 8%
where the time goes in v3:
time: 81.4 us; the launch traced here: 81.3 us
  blocking collectives  41.5 us (51%)
  Pallas kernels  14.4 us (18%)
  waiting for transfers between devices  13.8 us (17%)
  starting transfers between devices  11.5 us (14%)
    all_to_all x1, blocking collectives, shards(): lax.all_to_all(outbound, 'ep', split_axis=0, concat_axis=0, tiled=True)  24.6 us
    all_to_all x1, blocking collectives, shards(): lax.all_to_all(summed, 'ep', split_axis=0, concat_axis=0, tiled=True)  16.8 us
    ppermute x12, waiting for transfers between devices, passed_on(): lax.ppermute(shard, 'tp', [(i, (i + step) % devices) for i in range(devic...  13.8 us
    ppermute x12, starting transfers between devices, passed_on(): lax.ppermute(shard, 'tp', [(i, (i + step) % devices) for i in range(devic...  11.5 us
    pallas_call x1, Pallas kernels, attend(): pl.pallas_call(attention_kernel, name='attend', compiler_params=pltpu.Com...  6.04 us
    pallas_call x1, Pallas kernels, dense_branch(): pl.pallas_call(dense_kernel, name='dense', compiler_params=pltpu.Compiler...  3.13 us
    pallas_call x1, Pallas kernels, load(): pl.pallas_call(load_kernel, name='load', compiler_params=pltpu.CompilerPa...  3.02 us
  transfers between devices with their start and end apart: 12, of which 6 were waited for; matrix products, arithmetic and copies ran while one was open for 0% of the time, Pallas kernels for 8%

profile of v3, /device:TPU:1, one launch (start us, length us, event | category | flops | bytes accessed | tf_op | source)
XLA Modules:
  0.0 81.3 jit_solution(14884257596482223500)
XLA Ops:
  0.0 6.0 %attend.1.refs_0_.own = bf16[16,2048]{1,0:T(8,128)(2,1)S(1)} custom-call(s32[16]{0:T(128)} %lengths_hbm.1, f32[2]{0:T(128)} %lambdas_hbm.1, bf16[16,2048]{1,0:T(8,128)(2,1)} %refs_3_.1, f32[1,2048]{1,0:T(1,128)} %bitcast.17, f32[1,128]{1,0:T(1,128)} %bitcast.21, bf16[2048,256]{1,0:T(8,128)(2,1)} %query_hbm.1, bf16[2048,128]{1,0:T(8,128)(2,1)} %key_hbm.1, ...), custom_call_target="tpu_custom_call" | custom-call | tf_op jit(solution)/shard_map/attend/pallas_call | solution.py:159
  6.0 3.4 %collective-permute-start.2 = (bf16[16,2048]{1,0:T(8,128)(2,1)S(1)}, bf16[16,2048]{1,0:T(8,128)(2,1)S(1)}, u32[]{:S(2)}, u32[]{:S(2)}) collective-permute-start(bf16[16,2048]{1,0:T(8,128)(2,1)S(1)} %attend.1.refs_0_.own), channel_id=1, source_target_pairs={{0,3},{1,0},{2,1},{3,2},{4,7},{5,4},{6,5},{7,6},{8,11},{9,8},{10,9... | collective-permute-start | bytes 196616 | tf_op jit(solution)/shard_map/ppermute | solution.py:418
  9.4 0.5 collective-permute-start.1
  9.9 0.6 collective-permute-start
  10.5 3.0 %load.1 = (s32[4,16]{1,0:T(4,128)S(1)}, f32[4,16]{1,0:T(4,128)S(1)}, bf16[16,2048]{1,0:T(8,128)(2,1)S(1)}, f32[1,2048]{1,0:T(1,128)S(1)}, f32[1,512]{1,0:T(1,128...) custom-call(bf16[16,2048]{1,0:T(8,128)(2,1)S(1)} %attend.1.refs_0_.own, ...), custom_call_target="tpu_custom_call" | custom-call | flops 1073741824 | bytes 6367744 | tf_op jit(solution)/shard_map/load/pallas_call | solution.py:190
  13.6 0.2 plan.1
  13.7 0.3 collective-permute-done.1.two
  14.1 0.7 collective-permute-done.one
  14.7 0.3 normalise.1
  15.1 24.6 %all_to_all.10.own = bf16[64,2,512]{2,1,0:T(2,128)(2,1)S(1)} all-to-all(bf16[64,2,512]{2,1,0:T(2,128)(2,1)S(1)} %get-tuple-element.38), channel_id=1, replica_groups=mesh['ep'=64,'tp'=4] {'ep'}, dimensions={0} | all-to-all | bytes 262144 | tf_op jit(solution)/shard_map/all_to_all | solution.py:468
  39.7 0.5 collective-permute-start.5
  40.2 1.2 %collective-permute-start.4 = (bf16[64,2,512]{2,1,0:T(2,128)(2,1)S(1)}, bf16[64,2,512]{2,1,0:T(2,128)(2,1)S(1)}, u32[]{:S(2)}, u32[]{:S(2)}) collective-permute-start(bf16[64,2,512]{2,1,0:T(2,128)(2,1)S(1)} %all_to_all.10.own), channel_id=1, source_target_pairs={{0,2},{1,3},{2,0},{3,1},{4,6},{5,7},{6,4},{7,5},{8,10},{9,11},{10,... | collective-permute-start | bytes 393224 | tf_op jit(solution)/shard_map/ppermute | solution.py:418
  41.5 0.2 collective-permute-start.3
  41.6 3.1 %dense.1 = (bf16[2048,256]{1,0:T(8,128)(2,1)S(1)}, bf16[2048,256]{1,0:T(8,128)(2,1)S(1)}, bf16[256,2048]{1,0:T(8,128)(2,1)S(1)}, bf16[32,512]{1,0:T(8,128)(2,1)S...) custom-call(bf16[16,2048]{1,0:T(8,128)(2,1)S(1)} %get-tuple-element.41.rows, ...), custom_call_target="tpu_custom_call" | custom-call | flops 100663296 | bytes 6291456 | tf_op jit(solution)/shard_map/dense/pallas_call | solution.py:311
  44.8 1.3 %collective-permute-done.4.two = bf16[64,2,512]{2,1,0:T(2,128)(2,1)S(1)} collective-permute-done((bf16[64,2,512]{2,1,0:T(2,128)(2,1)S(1)}, bf16[64,2,512]{2,1,0:T(2,128)(2,1)S(1)}, u32[]{:S(2)}, u32[]{:S(2)}) %collective-permute-start.4) | collective-permute-done | bytes 131104 | tf_op jit(solution)/shard_map/ppermute | solution.py:418
  46.1 3.6 %collective-permute-done.3.one = bf16[64,2,512]{2,1,0:T(2,128)(2,1)S(1)} collective-permute-done((bf16[64,2,512]{2,1,0:T(2,128)(2,1)S(1)}, bf16[64,2,512]{2,1,0:T(2,128)(2,1)S(1)}, u32[]{:S(2)}, u32[]{:S(2)}) %collective-permute-start.3) | collective-permute-done | bytes 131104 | tf_op jit(solution)/shard_map/ppermute | solution.py:418
  49.7 0.7 experts.1
  50.5 1.6 %collective-permute-start.7 = (bf16[128,512]{1,0:T(8,128)(2,1)S(1)}, bf16[128,512]{1,0:T(8,128)(2,1)S(1)}, u32[]{:S(2)}, u32[]{:S(2)}) collective-permute-start(bf16[128,512]{1,0:T(8,128)(2,1)S(1)} %get-tuple-element.51), channel_id=1, source_target_pairs={{0,2},{1,3},{2,0},{3,1},{4,6},{5,7},{6,4},{7,5},{8,10},{9,11},{10,... | collective-permute-start | bytes 393224 | tf_op jit(solution)/shard_map/ppermute | solution.py:418
  52.1 2.0 %collective-permute-start.8 = (bf16[128,512]{1,0:T(8,128)(2,1)S(1)}, bf16[128,512]{1,0:T(8,128)(2,1)S(1)}, u32[]{:S(2)}, u32[]{:S(2)}) collective-permute-start(bf16[128,512]{1,0:T(8,128)(2,1)S(1)} %get-tuple-element.52), channel_id=1, source_target_pairs={{0,3},{1,0},{2,1},{3,2},{4,7},{5,4},{6,5},{7,6},{8,11},{9,8},{10,9... | collective-permute-start | bytes 393224 | tf_op jit(solution)/shard_map/ppermute | solution.py:418
  54.1 1.5 %collective-permute-start.10 = (bf16[32,512]{1,0:T(8,128)(2,1)S(1)}, bf16[32,512]{1,0:T(8,128)(2,1)S(1)}, u32[]{:S(2)}, u32[]{:S(2)}) collective-permute-start(bf16[32,512]{1,0:T(8,128)(2,1)S(1)} %get-tuple-element.55), channel_id=1, source_target_pairs={{0,2},{1,3},{2,0},{3,1},{4,6},{5,7},{6,4},{7,5},{8,10},{9,11},{10,... | collective-permute-start | bytes 98312 | tf_op jit(solution)/shard_map/ppermute | solution.py:418
  55.6 5.1 %collective-permute-done.9.dense_one = bf16[32,512]{1,0:T(8,128)(2,1)S(1)} collective-permute-done((bf16[32,512]{1,0:T(8,128)(2,1)S(1)}, bf16[32,512]{1,0:T(8,128)(2,1)S(1)}, u32[]{:S(2)}, u32[]{:S(2)}) %collective-permute-start.9) | collective-permute-done | bytes 32800 | tf_op jit(solution)/shard_map/ppermute | solution.py:418
  60.7 2.8 %collective-permute-done.11.dense_three = bf16[32,512]{1,0:T(8,128)(2,1)S(1)} collective-permute-done((bf16[32,512]{1,0:T(8,128)(2,1)S(1)}, bf16[32,512]{1,0:T(8,128)(2,1)S(1)}, u32[]{:S(2)}, u32[]{:S(2)}) %collective-permute-start.11) | collective-permute-done | bytes 32800 | tf_op jit(solution)/shard_map/ppermute | solution.py:418
  63.6 16.8 %all_to_all.11.returned = bf16[64,2,512]{2,1,0:T(2,128)(2,1)S(1)} all-to-all(bf16[64,2,512]{2,1,0:T(2,128)(2,1)S(1)} %get-tuple-element.60), channel_id=1, replica_groups=mesh['ep'=64,'tp'=4] {'ep'}, dimensions={0} | all-to-all | bytes 262144 | tf_op jit(solution)/shard_map/all_to_all | solution.py:481
  80.4 0.9 %combine.1 = bf16[16,512]{1,0:T(8,128)(2,1)} custom-call(f32[16,512]{1,0:T(8,128)S(1)} %get-tuple-element.58.kept, f32[128,16]{1,0:T(8,128)S(1)} %get-tuple-element.59.mix, bf16[64,2,512]{2,1,0:T(2,128)(2,1)S(1)} %all_to_all.11.returned), custom_call_target="tpu_custom_call" | custom-call | tf_op jit(solution)/shard_map/combine/pallas_call | solution.py:406
  (10 shorter events, 0.2 us)
Async XLA Ops:
  6.0 7.7 %collective-permute-start.2 = (bf16[16,2048]{1,0:T(8,128)(2,1)S(1)}, bf16[16,2048]{1,0:T(8,128)(2,1)S(1)}, u32[]{:S(2)}, u32[]{:S(2)}) collective-permute-start(bf16[16,2048]{1,0:T(8,128)(2,1)S(1)} %attend.1.refs_0_.own), channel_id=1, source_target_pairs={{0,3},{1,0},{2,1},{3,2},{4,7},{5,4},{6,5},{7,6},{8,11},{9,8},{10,9... | collective-permute-start | bytes 196616 | tf_op jit(solution)/shard_map/ppermute | solution.py:418
  9.4 4.7 %collective-permute-start.1 = (bf16[16,2048]{1,0:T(8,128)(2,1)S(1)}, bf16[16,2048]{1,0:T(8,128)(2,1)S(1)}, u32[]{:S(2)}, u32[]{:S(2)}) collective-permute-start(bf16[16,2048]{1,0:T(8,128)(2,1)S(1)} %attend.1.refs_0_.own), channel_id=1, source_target_pairs={{0,2},{1,3},{2,0},{3,1},{4,6},{5,7},{6,4},{7,5},{8,10},{9,11},{10,... | collective-permute-start | bytes 196616 | tf_op jit(solution)/shard_map/ppermute | solution.py:418
  9.9 4.8 %collective-permute-start = (bf16[16,2048]{1,0:T(8,128)(2,1)S(1)}, bf16[16,2048]{1,0:T(8,128)(2,1)S(1)}, u32[]{:S(2)}, u32[]{:S(2)}) collective-permute-start(bf16[16,2048]{1,0:T(8,128)(2,1)S(1)} %attend.1.refs_0_.own), channel_id=1, source_target_pairs={{0,1},{1,2},{2,3},{3,0},{4,5},{5,6},{6,7},{7,4},{8,9},{9,10},{10,1... | collective-permute-start | bytes 196616 | tf_op jit(solution)/shard_map/ppermute | solution.py:418
  39.7 5.0 %collective-permute-start.5 = (bf16[64,2,512]{2,1,0:T(2,128)(2,1)S(1)}, bf16[64,2,512]{2,1,0:T(2,128)(2,1)S(1)}, u32[]{:S(2)}, u32[]{:S(2)}) collective-permute-start(bf16[64,2,512]{2,1,0:T(2,128)(2,1)S(1)} %all_to_all.10.own), channel_id=1, source_target_pairs={{0,3},{1,0},{2,1},{3,2},{4,7},{5,4},{6,5},{7,6},{8,11},{9,8},{10,9... | collective-permute-start | bytes 393224 | tf_op jit(solution)/shard_map/ppermute | solution.py:418
  40.2 5.9 %collective-permute-start.4 = (bf16[64,2,512]{2,1,0:T(2,128)(2,1)S(1)}, bf16[64,2,512]{2,1,0:T(2,128)(2,1)S(1)}, u32[]{:S(2)}, u32[]{:S(2)}) collective-permute-start(bf16[64,2,512]{2,1,0:T(2,128)(2,1)S(1)} %all_to_all.10.own), channel_id=1, source_target_pairs={{0,2},{1,3},{2,0},{3,1},{4,6},{5,7},{6,4},{7,5},{8,10},{9,11},{10,... | collective-permute-start | bytes 393224 | tf_op jit(solution)/shard_map/ppermute | solution.py:418
  41.5 8.2 %collective-permute-start.3 = (bf16[64,2,512]{2,1,0:T(2,128)(2,1)S(1)}, bf16[64,2,512]{2,1,0:T(2,128)(2,1)S(1)}, u32[]{:S(2)}, u32[]{:S(2)}) collective-permute-start(bf16[64,2,512]{2,1,0:T(2,128)(2,1)S(1)} %all_to_all.10.own), channel_id=1, source_target_pairs={{0,1},{1,2},{2,3},{3,0},{4,5},{5,6},{6,7},{7,4},{8,9},{9,10},{10,1... | collective-permute-start | bytes 393224 | tf_op jit(solution)/shard_map/ppermute | solution.py:418
  50.4 13.0 %collective-permute-start.6 = (bf16[128,512]{1,0:T(8,128)(2,1)S(1)}, bf16[128,512]{1,0:T(8,128)(2,1)S(1)}, u32[]{:S(2)}, u32[]{:S(2)}) collective-permute-start(bf16[128,512]{1,0:T(8,128)(2,1)S(1)} %get-tuple-element.50), channel_id=1, source_target_pairs={{0,1},{1,2},{2,3},{3,0},{4,5},{5,6},{6,7},{7,4},{8,9},{9,10},{10,1... | collective-permute-start | bytes 393224 | tf_op jit(solution)/shard_map/ppermute | solution.py:418
  50.5 12.9 %collective-permute-start.7 = (bf16[128,512]{1,0:T(8,128)(2,1)S(1)}, bf16[128,512]{1,0:T(8,128)(2,1)S(1)}, u32[]{:S(2)}, u32[]{:S(2)}) collective-permute-start(bf16[128,512]{1,0:T(8,128)(2,1)S(1)} %get-tuple-element.51), channel_id=1, source_target_pairs={{0,2},{1,3},{2,0},{3,1},{4,6},{5,7},{6,4},{7,5},{8,10},{9,11},{10,... | collective-permute-start | bytes 393224 | tf_op jit(solution)/shard_map/ppermute | solution.py:418
  52.1 11.3 %collective-permute-start.8 = (bf16[128,512]{1,0:T(8,128)(2,1)S(1)}, bf16[128,512]{1,0:T(8,128)(2,1)S(1)}, u32[]{:S(2)}, u32[]{:S(2)}) collective-permute-start(bf16[128,512]{1,0:T(8,128)(2,1)S(1)} %get-tuple-element.52), channel_id=1, source_target_pairs={{0,3},{1,0},{2,1},{3,2},{4,7},{5,4},{6,5},{7,6},{8,11},{9,8},{10,9... | collective-permute-start | bytes 393224 | tf_op jit(solution)/shard_map/ppermute | solution.py:418
  54.1 6.6 %collective-permute-start.9 = (bf16[32,512]{1,0:T(8,128)(2,1)S(1)}, bf16[32,512]{1,0:T(8,128)(2,1)S(1)}, u32[]{:S(2)}, u32[]{:S(2)}) collective-permute-start(bf16[32,512]{1,0:T(8,128)(2,1)S(1)} %get-tuple-element.54), channel_id=1, source_target_pairs={{0,1},{1,2},{2,3},{3,0},{4,5},{5,6},{6,7},{7,4},{8,9},{9,10},{10,1... | collective-permute-start | bytes 98312 | tf_op jit(solution)/shard_map/ppermute | solution.py:418
  54.1 6.6 %collective-permute-start.10 = (bf16[32,512]{1,0:T(8,128)(2,1)S(1)}, bf16[32,512]{1,0:T(8,128)(2,1)S(1)}, u32[]{:S(2)}, u32[]{:S(2)}) collective-permute-start(bf16[32,512]{1,0:T(8,128)(2,1)S(1)} %get-tuple-element.55), channel_id=1, source_target_pairs={{0,2},{1,3},{2,0},{3,1},{4,6},{5,7},{6,4},{7,5},{8,10},{9,11},{10,... | collective-permute-start | bytes 98312 | tf_op jit(solution)/shard_map/ppermute | solution.py:418
  60.7 2.8 %collective-permute-start.11 = (bf16[32,512]{1,0:T(8,128)(2,1)S(1)}, bf16[32,512]{1,0:T(8,128)(2,1)S(1)}, u32[]{:S(2)}, u32[]{:S(2)}) collective-permute-start(bf16[32,512]{1,0:T(8,128)(2,1)S(1)} %get-tuple-element.56), channel_id=1, source_target_pairs={{0,3},{1,0},{2,1},{3,2},{4,7},{5,4},{6,5},{7,6},{8,11},{9,8},{10,9... | collective-permute-start | bytes 98312 | tf_op jit(solution)/shard_map/ppermute | solution.py:418

commit v4 on v3

--- a/solution.py
+++ b/solution.py
@@ -10,7 +10,7 @@
 DV = 128
 TOPK = 4
 CAP = 2
-GROUP = 4
+GROUP = 8
 
 epsilon = 1e-06
 F32 = jnp.float32
@@ -218,10 +218,18 @@
     return jnp.where(chosen, named, 0.0), jnp.where(chosen, weighed, 0.0)
 
 
+def three_pieces(values):
+    high = values.astype(BF16)
+    rest = values - high.astype(F32)
+    middle = rest.astype(BF16)
+    return high, middle, (rest - middle.astype(F32)).astype(BF16)
+
+
 def plan_kernel(routes, route_weight, dispatch, mix):
     named, weighed = slot_masks(routes, route_weight, dispatch.shape[0])
     dispatch[...] = named.astype(BF16)
-    mix[...] = weighed
+    for i, piece in enumerate(three_pieces(weighed.T)):
+        mix[i] = piece
 
 
 def plan(routes, route_weight, slots):
@@ -230,7 +238,7 @@
         plan_kernel,
         name="plan",
         compiler_params=pltpu.CompilerParams(vmem_limit_bytes=4 << 20),
-        out_shape=(pltpu.VMEM((slots, seq_count), BF16), pltpu.VMEM((slots, seq_count), F32)),
+        out_shape=(pltpu.VMEM((slots, seq_count), BF16), pltpu.VMEM((3, seq_count, slots), BF16)),
         in_specs=whole(2),
         out_specs=tuple(whole(2)),
         cost_estimate=pl.CostEstimate(flops=1 << 28, bytes_accessed=1 << 10, transcendentals=0),
@@ -288,10 +296,7 @@
     up_proj = dot(value, up[...], ((1,), (1,)))
     hidden = (silu(gate_pre) * up_proj).astype(BF16)
     part = jnp.sum(hidden.astype(F32) * vector[...], axis=1, keepdims=True)
-    high = part.astype(BF16)
-    rest = part - high.astype(F32)
-    middle = rest.astype(BF16)
-    low = (rest - middle.astype(F32)).astype(BF16)
+    high, middle, low = three_pieces(part)
     lane = lax.broadcasted_iota(jnp.int32, (seq_count, columns), 1)
     pieces = jnp.where(
         lane == 0, high.astype(F32), jnp.where(lane == 1, middle.astype(F32), low.astype(F32))
@@ -392,13 +397,8 @@
 
 
 def combine_kernel(kept, mix, returned, out):
-    picked = lax.dot_general(
-        mix[...],
-        returned[...].reshape(mix.shape[0], -1).astype(F32),
-        (((0,), (0,)), ((), ())),
-        precision=lax.Precision.HIGHEST,
-        preferred_element_type=F32,
-    )
+    rows = returned[...].reshape(mix.shape[2], -1)
+    picked = dot(mix[0], rows) + (dot(mix[1], rows) + dot(mix[2], rows))
     out[...] = (kept[...] + picked).astype(BF16)
 
 

time: 81.4 us -> 80.6 us (level)
  Pallas kernels: 14.4 us -> 13.5 us
where the time goes in v4:
time: 80.6 us; the launch traced here: 80.4 us
  blocking collectives  41.5 us (51%)
  waiting for transfers between devices  13.8 us (17%)
  Pallas kernels  13.5 us (17%)
  starting transfers between devices  11.5 us (14%)
    all_to_all x1, blocking collectives, shards(): lax.all_to_all(outbound, 'ep', split_axis=0, concat_axis=0, tiled=True)  24.6 us
    all_to_all x1, blocking collectives, shards(): lax.all_to_all(summed, 'ep', split_axis=0, concat_axis=0, tiled=True)  16.8 us
    ppermute x12, waiting for transfers between devices, passed_on(): lax.ppermute(shard, 'tp', [(i, (i + step) % devices) for i in range(devic...  13.8 us
    ppermute x12, starting transfers between devices, passed_on(): lax.ppermute(shard, 'tp', [(i, (i + step) % devices) for i in range(devic...  11.5 us
    pallas_call x1, Pallas kernels, attend(): pl.pallas_call(attention_kernel, name='attend', compiler_params=pltpu.Com...  5.25 us
    pallas_call x1, Pallas kernels, dense_branch(): pl.pallas_call(dense_kernel, name='dense', compiler_params=pltpu.Compiler...  3.13 us
    pallas_call x1, Pallas kernels, load(): pl.pallas_call(load_kernel, name='load', compiler_params=pltpu.CompilerPa...  3.02 us
  transfers between devices with their start and end apart: 12, of which 6 were waited for; matrix products, arithmetic and copies ran while one was open for 0% of the time, Pallas kernels for 8%

profile of v4, /device:TPU:1, one launch (start us, length us, event | category | flops | bytes accessed | tf_op | source)
XLA Modules:
  0.0 80.4 jit_solution(11199853056368492244)
XLA Ops:
  0.0 5.3 %attend.1.refs_0_.own = bf16[16,2048]{1,0:T(8,128)(2,1)S(1)} custom-call(s32[16]{0:T(128)} %lengths_hbm.1, f32[2]{0:T(128)} %lambdas_hbm.1, bf16[16,2048]{1,0:T(8,128)(2,1)} %refs_3_.1, f32[1,2048]{1,0:T(1,128)} %bitcast.17, f32[1,128]{1,0:T(1,128)} %bitcast.21, bf16[2048,256]{1,0:T(8,128)(2,1)} %query_hbm.1, bf16[2048,128]{1,0:T(8,128)(2,1)} %key_hbm.1, ...), custom_call_target="tpu_custom_call" | custom-call | tf_op jit(solution)/shard_map/attend/pallas_call | solution.py:159
  5.3 3.4 %collective-permute-start.2 = (bf16[16,2048]{1,0:T(8,128)(2,1)S(1)}, bf16[16,2048]{1,0:T(8,128)(2,1)S(1)}, u32[]{:S(2)}, u32[]{:S(2)}) collective-permute-start(bf16[16,2048]{1,0:T(8,128)(2,1)S(1)} %attend.1.refs_0_.own), channel_id=1, source_target_pairs={{0,3},{1,0},{2,1},{3,2},{4,7},{5,4},{6,5},{7,6},{8,11},{9,8},{10,9... | collective-permute-start | bytes 196616 | tf_op jit(solution)/shard_map/ppermute | solution.py:418
  8.6 0.5 collective-permute-start.1
  9.2 0.6 collective-permute-start
  9.8 3.0 %load.1 = (s32[4,16]{1,0:T(4,128)S(1)}, f32[4,16]{1,0:T(4,128)S(1)}, bf16[16,2048]{1,0:T(8,128)(2,1)S(1)}, f32[1,2048]{1,0:T(1,128)S(1)}, f32[1,512]{1,0:T(1,128...) custom-call(bf16[16,2048]{1,0:T(8,128)(2,1)S(1)} %attend.1.refs_0_.own, ...), custom_call_target="tpu_custom_call" | custom-call | flops 1073741824 | bytes 6367744 | tf_op jit(solution)/shard_map/load/pallas_call | solution.py:190
  12.8 0.2 plan.1
  13.0 0.3 collective-permute-done.1.two
  13.3 0.7 collective-permute-done.one
  14.0 0.3 normalise.1
  14.3 24.6 %all_to_all.10.own = bf16[64,2,512]{2,1,0:T(2,128)(2,1)S(1)} all-to-all(bf16[64,2,512]{2,1,0:T(2,128)(2,1)S(1)} %get-tuple-element.38), channel_id=1, replica_groups=mesh['ep'=64,'tp'=4] {'ep'}, dimensions={0} | all-to-all | bytes 262144 | tf_op jit(solution)/shard_map/all_to_all | solution.py:468
  38.9 0.5 collective-permute-start.5
  39.5 1.2 %collective-permute-start.4 = (bf16[64,2,512]{2,1,0:T(2,128)(2,1)S(1)}, bf16[64,2,512]{2,1,0:T(2,128)(2,1)S(1)}, u32[]{:S(2)}, u32[]{:S(2)}) collective-permute-start(bf16[64,2,512]{2,1,0:T(2,128)(2,1)S(1)} %all_to_all.10.own), channel_id=1, source_target_pairs={{0,2},{1,3},{2,0},{3,1},{4,6},{5,7},{6,4},{7,5},{8,10},{9,11},{10,... | collective-permute-start | bytes 393224 | tf_op jit(solution)/shard_map/ppermute | solution.py:418
  40.7 0.1 collective-permute-start.3
  40.8 3.1 %dense.1 = (bf16[2048,256]{1,0:T(8,128)(2,1)S(1)}, bf16[2048,256]{1,0:T(8,128)(2,1)S(1)}, bf16[256,2048]{1,0:T(8,128)(2,1)S(1)}, bf16[32,512]{1,0:T(8,128)(2,1)S...) custom-call(bf16[16,2048]{1,0:T(8,128)(2,1)S(1)} %get-tuple-element.41.rows, ...), custom_call_target="tpu_custom_call" | custom-call | flops 100663296 | bytes 6291456 | tf_op jit(solution)/shard_map/dense/pallas_call | solution.py:316
  44.0 1.4 %collective-permute-done.4.two = bf16[64,2,512]{2,1,0:T(2,128)(2,1)S(1)} collective-permute-done((bf16[64,2,512]{2,1,0:T(2,128)(2,1)S(1)}, bf16[64,2,512]{2,1,0:T(2,128)(2,1)S(1)}, u32[]{:S(2)}, u32[]{:S(2)}) %collective-permute-start.4) | collective-permute-done | bytes 131104 | tf_op jit(solution)/shard_map/ppermute | solution.py:418
  45.4 3.6 %collective-permute-done.3.one = bf16[64,2,512]{2,1,0:T(2,128)(2,1)S(1)} collective-permute-done((bf16[64,2,512]{2,1,0:T(2,128)(2,1)S(1)}, bf16[64,2,512]{2,1,0:T(2,128)(2,1)S(1)}, u32[]{:S(2)}, u32[]{:S(2)}) %collective-permute-start.3) | collective-permute-done | bytes 131104 | tf_op jit(solution)/shard_map/ppermute | solution.py:418
  49.0 0.7 experts.1
  49.8 1.6 %collective-permute-start.7 = (bf16[128,512]{1,0:T(8,128)(2,1)S(1)}, bf16[128,512]{1,0:T(8,128)(2,1)S(1)}, u32[]{:S(2)}, u32[]{:S(2)}) collective-permute-start(bf16[128,512]{1,0:T(8,128)(2,1)S(1)} %get-tuple-element.51), channel_id=1, source_target_pairs={{0,2},{1,3},{2,0},{3,1},{4,6},{5,7},{6,4},{7,5},{8,10},{9,11},{10,... | collective-permute-start | bytes 393224 | tf_op jit(solution)/shard_map/ppermute | solution.py:418
  51.4 2.0 %collective-permute-start.8 = (bf16[128,512]{1,0:T(8,128)(2,1)S(1)}, bf16[128,512]{1,0:T(8,128)(2,1)S(1)}, u32[]{:S(2)}, u32[]{:S(2)}) collective-permute-start(bf16[128,512]{1,0:T(8,128)(2,1)S(1)} %get-tuple-element.52), channel_id=1, source_target_pairs={{0,3},{1,0},{2,1},{3,2},{4,7},{5,4},{6,5},{7,6},{8,11},{9,8},{10,9... | collective-permute-start | bytes 393224 | tf_op jit(solution)/shard_map/ppermute | solution.py:418
  53.3 1.5 %collective-permute-start.10 = (bf16[32,512]{1,0:T(8,128)(2,1)S(1)}, bf16[32,512]{1,0:T(8,128)(2,1)S(1)}, u32[]{:S(2)}, u32[]{:S(2)}) collective-permute-start(bf16[32,512]{1,0:T(8,128)(2,1)S(1)} %get-tuple-element.55), channel_id=1, source_target_pairs={{0,2},{1,3},{2,0},{3,1},{4,6},{5,7},{6,4},{7,5},{8,10},{9,11},{10,... | collective-permute-start | bytes 98312 | tf_op jit(solution)/shard_map/ppermute | solution.py:418
  54.8 5.1 %collective-permute-done.9.dense_one = bf16[32,512]{1,0:T(8,128)(2,1)S(1)} collective-permute-done((bf16[32,512]{1,0:T(8,128)(2,1)S(1)}, bf16[32,512]{1,0:T(8,128)(2,1)S(1)}, u32[]{:S(2)}, u32[]{:S(2)}) %collective-permute-start.9) | collective-permute-done | bytes 32800 | tf_op jit(solution)/shard_map/ppermute | solution.py:418
  59.9 2.8 %collective-permute-done.11.dense_three = bf16[32,512]{1,0:T(8,128)(2,1)S(1)} collective-permute-done((bf16[32,512]{1,0:T(8,128)(2,1)S(1)}, bf16[32,512]{1,0:T(8,128)(2,1)S(1)}, u32[]{:S(2)}, u32[]{:S(2)}) %collective-permute-start.11) | collective-permute-done | bytes 32800 | tf_op jit(solution)/shard_map/ppermute | solution.py:418
  62.8 16.8 %all_to_all.11.returned = bf16[64,2,512]{2,1,0:T(2,128)(2,1)S(1)} all-to-all(bf16[64,2,512]{2,1,0:T(2,128)(2,1)S(1)} %get-tuple-element.60), channel_id=1, replica_groups=mesh['ep'=64,'tp'=4] {'ep'}, dimensions={0} | all-to-all | bytes 262144 | tf_op jit(solution)/shard_map/all_to_all | solution.py:481
  79.6 0.8 combine.1
  (10 shorter events, 0.2 us)
Async XLA Ops:
  5.3 7.7 %collective-permute-start.2 = (bf16[16,2048]{1,0:T(8,128)(2,1)S(1)}, bf16[16,2048]{1,0:T(8,128)(2,1)S(1)}, u32[]{:S(2)}, u32[]{:S(2)}) collective-permute-start(bf16[16,2048]{1,0:T(8,128)(2,1)S(1)} %attend.1.refs_0_.own), channel_id=1, source_target_pairs={{0,3},{1,0},{2,1},{3,2},{4,7},{5,4},{6,5},{7,6},{8,11},{9,8},{10,9... | collective-permute-start | bytes 196616 | tf_op jit(solution)/shard_map/ppermute | solution.py:418
  8.6 4.7 %collective-permute-start.1 = (bf16[16,2048]{1,0:T(8,128)(2,1)S(1)}, bf16[16,2048]{1,0:T(8,128)(2,1)S(1)}, u32[]{:S(2)}, u32[]{:S(2)}) collective-permute-start(bf16[16,2048]{1,0:T(8,128)(2,1)S(1)} %attend.1.refs_0_.own), channel_id=1, source_target_pairs={{0,2},{1,3},{2,0},{3,1},{4,6},{5,7},{6,4},{7,5},{8,10},{9,11},{10,... | collective-permute-start | bytes 196616 | tf_op jit(solution)/shard_map/ppermute | solution.py:418
  9.2 4.8 %collective-permute-start = (bf16[16,2048]{1,0:T(8,128)(2,1)S(1)}, bf16[16,2048]{1,0:T(8,128)(2,1)S(1)}, u32[]{:S(2)}, u32[]{:S(2)}) collective-permute-start(bf16[16,2048]{1,0:T(8,128)(2,1)S(1)} %attend.1.refs_0_.own), channel_id=1, source_target_pairs={{0,1},{1,2},{2,3},{3,0},{4,5},{5,6},{6,7},{7,4},{8,9},{9,10},{10,1... | collective-permute-start | bytes 196616 | tf_op jit(solution)/shard_map/ppermute | solution.py:418
  38.9 5.1 %collective-permute-start.5 = (bf16[64,2,512]{2,1,0:T(2,128)(2,1)S(1)}, bf16[64,2,512]{2,1,0:T(2,128)(2,1)S(1)}, u32[]{:S(2)}, u32[]{:S(2)}) collective-permute-start(bf16[64,2,512]{2,1,0:T(2,128)(2,1)S(1)} %all_to_all.10.own), channel_id=1, source_target_pairs={{0,3},{1,0},{2,1},{3,2},{4,7},{5,4},{6,5},{7,6},{8,11},{9,8},{10,9... | collective-permute-start | bytes 393224 | tf_op jit(solution)/shard_map/ppermute | solution.py:418
  39.5 5.9 %collective-permute-start.4 = (bf16[64,2,512]{2,1,0:T(2,128)(2,1)S(1)}, bf16[64,2,512]{2,1,0:T(2,128)(2,1)S(1)}, u32[]{:S(2)}, u32[]{:S(2)}) collective-permute-start(bf16[64,2,512]{2,1,0:T(2,128)(2,1)S(1)} %all_to_all.10.own), channel_id=1, source_target_pairs={{0,2},{1,3},{2,0},{3,1},{4,6},{5,7},{6,4},{7,5},{8,10},{9,11},{10,... | collective-permute-start | bytes 393224 | tf_op jit(solution)/shard_map/ppermute | solution.py:418
  40.7 8.3 %collective-permute-start.3 = (bf16[64,2,512]{2,1,0:T(2,128)(2,1)S(1)}, bf16[64,2,512]{2,1,0:T(2,128)(2,1)S(1)}, u32[]{:S(2)}, u32[]{:S(2)}) collective-permute-start(bf16[64,2,512]{2,1,0:T(2,128)(2,1)S(1)} %all_to_all.10.own), channel_id=1, source_target_pairs={{0,1},{1,2},{2,3},{3,0},{4,5},{5,6},{6,7},{7,4},{8,9},{9,10},{10,1... | collective-permute-start | bytes 393224 | tf_op jit(solution)/shard_map/ppermute | solution.py:418
  49.7 13.0 %collective-permute-start.6 = (bf16[128,512]{1,0:T(8,128)(2,1)S(1)}, bf16[128,512]{1,0:T(8,128)(2,1)S(1)}, u32[]{:S(2)}, u32[]{:S(2)}) collective-permute-start(bf16[128,512]{1,0:T(8,128)(2,1)S(1)} %get-tuple-element.50), channel_id=1, source_target_pairs={{0,1},{1,2},{2,3},{3,0},{4,5},{5,6},{6,7},{7,4},{8,9},{9,10},{10,1... | collective-permute-start | bytes 393224 | tf_op jit(solution)/shard_map/ppermute | solution.py:418
  49.8 12.9 %collective-permute-start.7 = (bf16[128,512]{1,0:T(8,128)(2,1)S(1)}, bf16[128,512]{1,0:T(8,128)(2,1)S(1)}, u32[]{:S(2)}, u32[]{:S(2)}) collective-permute-start(bf16[128,512]{1,0:T(8,128)(2,1)S(1)} %get-tuple-element.51), channel_id=1, source_target_pairs={{0,2},{1,3},{2,0},{3,1},{4,6},{5,7},{6,4},{7,5},{8,10},{9,11},{10,... | collective-permute-start | bytes 393224 | tf_op jit(solution)/shard_map/ppermute | solution.py:418
  51.4 11.3 %collective-permute-start.8 = (bf16[128,512]{1,0:T(8,128)(2,1)S(1)}, bf16[128,512]{1,0:T(8,128)(2,1)S(1)}, u32[]{:S(2)}, u32[]{:S(2)}) collective-permute-start(bf16[128,512]{1,0:T(8,128)(2,1)S(1)} %get-tuple-element.52), channel_id=1, source_target_pairs={{0,3},{1,0},{2,1},{3,2},{4,7},{5,4},{6,5},{7,6},{8,11},{9,8},{10,9... | collective-permute-start | bytes 393224 | tf_op jit(solution)/shard_map/ppermute | solution.py:418
  53.3 6.6 %collective-permute-start.9 = (bf16[32,512]{1,0:T(8,128)(2,1)S(1)}, bf16[32,512]{1,0:T(8,128)(2,1)S(1)}, u32[]{:S(2)}, u32[]{:S(2)}) collective-permute-start(bf16[32,512]{1,0:T(8,128)(2,1)S(1)} %get-tuple-element.54), channel_id=1, source_target_pairs={{0,1},{1,2},{2,3},{3,0},{4,5},{5,6},{6,7},{7,4},{8,9},{9,10},{10,1... | collective-permute-start | bytes 98312 | tf_op jit(solution)/shard_map/ppermute | solution.py:418
  53.3 6.6 %collective-permute-start.10 = (bf16[32,512]{1,0:T(8,128)(2,1)S(1)}, bf16[32,512]{1,0:T(8,128)(2,1)S(1)}, u32[]{:S(2)}, u32[]{:S(2)}) collective-permute-start(bf16[32,512]{1,0:T(8,128)(2,1)S(1)} %get-tuple-element.55), channel_id=1, source_target_pairs={{0,2},{1,3},{2,0},{3,1},{4,6},{5,7},{6,4},{7,5},{8,10},{9,11},{10,... | collective-permute-start | bytes 98312 | tf_op jit(solution)/shard_map/ppermute | solution.py:418
  59.9 2.8 %collective-permute-start.11 = (bf16[32,512]{1,0:T(8,128)(2,1)S(1)}, bf16[32,512]{1,0:T(8,128)(2,1)S(1)}, u32[]{:S(2)}, u32[]{:S(2)}) collective-permute-start(bf16[32,512]{1,0:T(8,128)(2,1)S(1)} %get-tuple-element.56), channel_id=1, source_target_pairs={{0,3},{1,0},{2,1},{3,2},{4,7},{5,4},{6,5},{7,6},{8,11},{9,8},{10,9... | collective-permute-start | bytes 98312 | tf_op jit(solution)/shard_map/ppermute | solution.py:418

commit v5 on v4

--- a/solution.py
+++ b/solution.py
@@ -173,34 +173,6 @@
     )(*all_far(lengths, lambdas, *vectors))
 
 
-def load_kernel(*refs):
-    count = (len(refs) - 2) // 2
-    sems = refs[-1]
-    copies = [
-        pltpu.make_async_copy(refs[1 + i], refs[1 + count + i], sems.at[i]) for i in range(count)
-    ]
-    for copy in copies:
-        copy.start()
-    for copy in copies:
-        copy.wait()
-
-
-def load(after, *values):
-    size = sum(value.size * value.dtype.itemsize for value in values)
-    return pl.pallas_call(
-        load_kernel,
-        name="load",
-        compiler_params=pltpu.CompilerParams(vmem_limit_bytes=4 << 20),
-        out_shape=tuple(pltpu.VMEM(value.shape, value.dtype) for value in values),
-        in_specs=whole(1) + [pl.BlockSpec(memory_space=pltpu.HBM)] * len(values),
-        out_specs=tuple(whole(len(values))),
-        scratch_shapes=[pltpu.SemaphoreType.DMA((len(values),))],
-        cost_estimate=pl.CostEstimate(
-            flops=1 << 30, bytes_accessed=size, transcendentals=0
-        ),
-    )(near(after), *all_far(*values))
-
-
 def slot_masks(routes, route_weight, slots):
     seq_count = routes.shape[1]
     slot_ids = lax.broadcasted_iota(jnp.int32, (slots, seq_count), 0)
@@ -225,24 +197,52 @@
     return high, middle, (rest - middle.astype(F32)).astype(BF16)
 
 
-def plan_kernel(routes, route_weight, dispatch, mix):
+def load_kernel(after, routes_hbm, route_weight_hbm, *refs):
+    count = (len(refs) - 5) // 2
+    dispatch, mix = refs[count : count + 2]
+    routes, route_weight, sems = refs[2 * count + 2 :]
+    sources = (routes_hbm, route_weight_hbm, *refs[:count])
+    targets = (routes, route_weight, *refs[count + 2 : 2 * count + 2])
+    copies = [
+        pltpu.make_async_copy(source, target, sems.at[i])
+        for i, (source, target) in enumerate(zip(sources, targets))
+    ]
+    for copy in copies:
+        copy.start()
+    copies[0].wait()
+    copies[1].wait()
     named, weighed = slot_masks(routes, route_weight, dispatch.shape[0])
     dispatch[...] = named.astype(BF16)
     for i, piece in enumerate(three_pieces(weighed.T)):
         mix[i] = piece
-
-
-def plan(routes, route_weight, slots):
+    for copy in copies[2:]:
+        copy.wait()
+
+
+def load(after, routes, route_weight, slots, *values):
+    size = sum(value.size * value.dtype.itemsize for value in values)
     seq_count = routes.shape[1]
-    return pl.pallas_call(
-        plan_kernel,
-        name="plan",
+    outs = pl.pallas_call(
+        load_kernel,
+        name="load",
         compiler_params=pltpu.CompilerParams(vmem_limit_bytes=4 << 20),
-        out_shape=(pltpu.VMEM((slots, seq_count), BF16), pltpu.VMEM((3, seq_count, slots), BF16)),
-        in_specs=whole(2),
-        out_specs=tuple(whole(2)),
-        cost_estimate=pl.CostEstimate(flops=1 << 28, bytes_accessed=1 << 10, transcendentals=0),
-    )(*all_near(routes, route_weight))
+        out_shape=(
+            pltpu.VMEM((slots, seq_count), BF16),
+            pltpu.VMEM((3, seq_count, slots), BF16),
+            *[pltpu.VMEM(value.shape, value.dtype) for value in values],
+        ),
+        in_specs=whole(1) + [pl.BlockSpec(memory_space=pltpu.HBM)] * (2 + len(values)),
+        out_specs=tuple(whole(2 + len(values))),
+        scratch_shapes=[
+            pltpu.VMEM(routes.shape, routes.dtype),
+            pltpu.VMEM(route_weight.shape, route_weight.dtype),
+            pltpu.SemaphoreType.DMA((2 + len(values),)),
+        ],
+        cost_estimate=pl.CostEstimate(
+            flops=1 << 30, bytes_accessed=size, transcendentals=0
+        ),
+    )(near(after), *all_far(routes, route_weight, *values))
+    return outs
 
 
 def normalise_kernel(
@@ -281,7 +281,7 @@
 
 
 def dense_kernel(rows, gate, up, down, vector, *refs):
-    far, near_refs, blocks, sems = refs[:3], refs[3:6], refs[6:-1], refs[-1]
+    far, near_refs, blocks, sems = refs[:2], refs[2:4], refs[4:-1], refs[-1]
     copies = [
         pltpu.make_async_copy(source, target, sems.at[i])
         for i, (source, target) in enumerate(zip(far, near_refs))
@@ -319,16 +319,16 @@
         compiler_params=pltpu.CompilerParams(vmem_limit_bytes=8 << 20),
         out_shape=tuple(pltpu.VMEM(value.shape, value.dtype) for value in expert_weights)
         + (block,) * devices,
-        in_specs=whole(5) + [pl.BlockSpec(memory_space=pltpu.HBM)] * 3,
-        out_specs=tuple(whole(3 + devices)),
-        scratch_shapes=[pltpu.SemaphoreType.DMA((3,))],
+        in_specs=whole(5) + [pl.BlockSpec(memory_space=pltpu.HBM)] * 2,
+        out_specs=tuple(whole(2 + devices)),
+        scratch_shapes=[pltpu.SemaphoreType.DMA((2,))],
         cost_estimate=pl.CostEstimate(
             flops=6 * seq_count * width * gate.shape[0],
             bytes_accessed=6 * width * gate.shape[0],
             transcendentals=0,
         ),
     )(*all_near(rows, gate, up, down, vector), *all_far(*expert_weights))
-    return outs[:3], outs[3:]
+    return outs[:2], outs[2:]
 
 
 def expert_kernel(own, one, two, three, gate, up, down, *blocks):
@@ -455,13 +455,12 @@
     )
     parts = [partial] + [passed_on(partial, step) for step in range(1, devices)]
     (
-        route_rows, weight_rows, near_tokens, near_gain, near_gate_vector,
-        near_dense_gate, near_dense_up, near_dense_down,
+        dispatch, mix, near_tokens, near_gain, near_gate_vector,
+        near_dense_gate, near_dense_up, near_dense_down, near_expert_down,
     ) = load(
-        partial, routes.T, route_weight.T, tokens, ffn_gain[None], gate_vector[None],
-        dense_gate, dense_up, dense_down,
-    )
-    dispatch, mix = plan(route_rows, weight_rows, slots)
+        partial, routes.T, route_weight.T, slots, tokens, ffn_gain[None], gate_vector[None],
+        dense_gate, dense_up, dense_down, expert_down[0],
+    )
     residual, ffn_in, outbound = normalise(
         near_tokens, parts, near_gain, dispatch, columns
     )
@@ -470,12 +469,12 @@
     gathered = [arrived] + [passed_on(arrived, step) for step in range(1, devices)]
     expert_weights, dense_blocks = dense_branch(
         ffn_in, near_dense_gate, near_dense_up, near_dense_down, near_gate_vector,
-        (expert_gate[0], expert_up[0], expert_down[0]), devices,
+        (expert_gate[0], expert_up[0]), devices,
     )
     dense_moved = [dense_blocks[0]]
     for step in range(1, devices):
         dense_moved.append(passed_on(dense_blocks[step], step))
-    blocks = expert_rows(gathered, *expert_weights)
+    blocks = expert_rows(gathered, *expert_weights, near_expert_down)
     moved = [blocks[0]] + [passed_on(blocks[step], step) for step in range(1, devices)]
     summed, kept = gather_parts(moved, dense_moved, residual, slots)
     returned = lax.all_to_all(summed, "ep", split_axis=0, concat_axis=0, tiled=True)

time: 80.6 us -> 80.6 us (level)
  transfers between devices with their start and end apart: 12 -> 12, of which waited for: 6 -> 6; matrix products, arithmetic and copies ran while one was open for 0% -> 0% of each run, Pallas kernels for 8% -> 7%
where the time goes in v5:
time: 80.6 us; the launch traced here: 80.5 us
  blocking collectives  41.5 us (51%)
  waiting for transfers between devices  14.2 us (18%)
  Pallas kernels  13.2 us (16%)
  starting transfers between devices  11.5 us (14%)
    all_to_all x1, blocking collectives, shards(): lax.all_to_all(outbound, 'ep', split_axis=0, concat_axis=0, tiled=True)  24.6 us
    all_to_all x1, blocking collectives, shards(): lax.all_to_all(summed, 'ep', split_axis=0, concat_axis=0, tiled=True)  16.9 us
    ppermute x12, waiting for transfers between devices, passed_on(): lax.ppermute(shard, 'tp', [(i, (i + step) % devices) for i in range(devic...  14.2 us
    ppermute x12, starting transfers between devices, passed_on(): lax.ppermute(shard, 'tp', [(i, (i + step) % devices) for i in range(devic...  11.5 us
    pallas_call x1, Pallas kernels, attend(): pl.pallas_call(attention_kernel, name='attend', compiler_params=pltpu.Com...  5.25 us
    pallas_call x1, Pallas kernels, load(): pl.pallas_call(load_kernel, name='load', compiler_params=pltpu.CompilerPa...  3.27 us
    pallas_call x1, Pallas kernels, dense_branch(): pl.pallas_call(dense_kernel, name='dense', compiler_params=pltpu.Compiler...  2.73 us
  transfers between devices with their start and end apart: 12, of which 6 were waited for; matrix products, arithmetic and copies ran while one was open for 0% of the time, Pallas kernels for 7%

profile of v5, /device:TPU:1, one launch (start us, length us, event | category | flops | bytes accessed | tf_op | source)
XLA Modules:
  0.0 80.5 jit_solution(5178792266558560459)
XLA Ops:
  0.0 5.3 %attend.1.after.own = bf16[16,2048]{1,0:T(8,128)(2,1)S(1)} custom-call(s32[16]{0:T(128)} %lengths_hbm.1, f32[2]{0:T(128)} %lambdas_hbm.1, bf16[16,2048]{1,0:T(8,128)(2,1)} %refs_0_.1, f32[1,2048]{1,0:T(1,128)} %bitcast.17, f32[1,128]{1,0:T(1,128)} %bitcast.21, bf16[2048,256]{1,0:T(8,128)(2,1)} %query_hbm.1, bf16[2048,128]{1,0:T(8,128)(2,1)} %key_hbm.1, ...), custom_call_target="tpu_custom_call" | custom-call | tf_op jit(solution)/shard_map/attend/pallas_call | solution.py:159
  5.3 3.4 %collective-permute-start.2 = (bf16[16,2048]{1,0:T(8,128)(2,1)S(1)}, bf16[16,2048]{1,0:T(8,128)(2,1)S(1)}, u32[]{:S(2)}, u32[]{:S(2)}) collective-permute-start(bf16[16,2048]{1,0:T(8,128)(2,1)S(1)} %attend.1.after.own), channel_id=1, source_target_pairs={{0,3},{1,0},{2,1},{3,2},{4,7},{5,4},{6,5},{7,6},{8,11},{9,8},{10,9... | collective-permute-start | bytes 196616 | tf_op jit(solution)/shard_map/ppermute | solution.py:418
  8.6 0.5 collective-permute-start.1
  9.2 0.6 collective-permute-start
  9.8 3.3 %load.1 = (bf16[128,16]{1,0:T(8,128)(2,1)S(1)}, bf16[3,16,128]{2,1,0:T(8,128)(2,1)S(1)}, bf16[16,2048]{1,0:T(8,128)(2,1)S(1)}, f32[1,2048]{1,0:T(1,128)S(1)}, f3...) custom-call(bf16[16,2048]{1,0:T(8,128)(2,1)S(1)} %attend.1.after.own, ...), custom_call_target="tpu_custom_call" | custom-call | flops 1073741824 | bytes 7415808 | tf_op jit(solution)/shard_map/load/pallas_call | solution.py:225
  13.0 0.3 collective-permute-done.1.two
  13.3 0.7 collective-permute-done.one
  14.0 0.3 normalise.1
  14.3 24.6 %all_to_all.10.own = bf16[64,2,512]{2,1,0:T(2,128)(2,1)S(1)} all-to-all(bf16[64,2,512]{2,1,0:T(2,128)(2,1)S(1)} %get-tuple-element.34), channel_id=1, replica_groups=mesh['ep'=64,'tp'=4] {'ep'}, dimensions={0} | all-to-all | bytes 262144 | tf_op jit(solution)/shard_map/all_to_all | solution.py:467
  38.9 0.6 collective-permute-start.5
  39.5 1.2 %collective-permute-start.4 = (bf16[64,2,512]{2,1,0:T(2,128)(2,1)S(1)}, bf16[64,2,512]{2,1,0:T(2,128)(2,1)S(1)}, u32[]{:S(2)}, u32[]{:S(2)}) collective-permute-start(bf16[64,2,512]{2,1,0:T(2,128)(2,1)S(1)} %all_to_all.10.own), channel_id=1, source_target_pairs={{0,2},{1,3},{2,0},{3,1},{4,6},{5,7},{6,4},{7,5},{8,10},{9,11},{10,... | collective-permute-start | bytes 393224 | tf_op jit(solution)/shard_map/ppermute | solution.py:418
  40.8 2.7 %dense.1 = (bf16[2048,256]{1,0:T(8,128)(2,1)S(1)}, bf16[2048,256]{1,0:T(8,128)(2,1)S(1)}, bf16[32,512]{1,0:T(8,128)(2,1)S(1)}, bf16[32,512]{1,0:T(8,128)(2,1)S(1...) custom-call(bf16[16,2048]{1,0:T(8,128)(2,1)S(1)} %get-tuple-element.37.rows, ...), custom_call_target="tpu_custom_call" | custom-call | flops 100663296 | bytes 6291456 | tf_op jit(solution)/shard_map/dense/pallas_call | solution.py:316
  43.6 1.8 %collective-permute-done.4.two = bf16[64,2,512]{2,1,0:T(2,128)(2,1)S(1)} collective-permute-done((bf16[64,2,512]{2,1,0:T(2,128)(2,1)S(1)}, bf16[64,2,512]{2,1,0:T(2,128)(2,1)S(1)}, u32[]{:S(2)}, u32[]{:S(2)}) %collective-permute-start.4) | collective-permute-done | bytes 131104 | tf_op jit(solution)/shard_map/ppermute | solution.py:418
  45.4 3.6 %collective-permute-done.3.one = bf16[64,2,512]{2,1,0:T(2,128)(2,1)S(1)} collective-permute-done((bf16[64,2,512]{2,1,0:T(2,128)(2,1)S(1)}, bf16[64,2,512]{2,1,0:T(2,128)(2,1)S(1)}, u32[]{:S(2)}, u32[]{:S(2)}) %collective-permute-start.3) | collective-permute-done | bytes 131104 | tf_op jit(solution)/shard_map/ppermute | solution.py:418
  49.0 0.7 experts.1
  49.7 0.1 collective-permute-start.6
  49.8 1.6 %collective-permute-start.7 = (bf16[128,512]{1,0:T(8,128)(2,1)S(1)}, bf16[128,512]{1,0:T(8,128)(2,1)S(1)}, u32[]{:S(2)}, u32[]{:S(2)}) collective-permute-start(bf16[128,512]{1,0:T(8,128)(2,1)S(1)} %get-tuple-element.47), channel_id=1, source_target_pairs={{0,2},{1,3},{2,0},{3,1},{4,6},{5,7},{6,4},{7,5},{8,10},{9,11},{10,... | collective-permute-start | bytes 393224 | tf_op jit(solution)/shard_map/ppermute | solution.py:418
  51.4 2.0 %collective-permute-start.8 = (bf16[128,512]{1,0:T(8,128)(2,1)S(1)}, bf16[128,512]{1,0:T(8,128)(2,1)S(1)}, u32[]{:S(2)}, u32[]{:S(2)}) collective-permute-start(bf16[128,512]{1,0:T(8,128)(2,1)S(1)} %get-tuple-element.48), channel_id=1, source_target_pairs={{0,3},{1,0},{2,1},{3,2},{4,7},{5,4},{6,5},{7,6},{8,11},{9,8},{10,9... | collective-permute-start | bytes 393224 | tf_op jit(solution)/shard_map/ppermute | solution.py:418
  53.4 1.5 %collective-permute-start.10 = (bf16[32,512]{1,0:T(8,128)(2,1)S(1)}, bf16[32,512]{1,0:T(8,128)(2,1)S(1)}, u32[]{:S(2)}, u32[]{:S(2)}) collective-permute-start(bf16[32,512]{1,0:T(8,128)(2,1)S(1)} %get-tuple-element.51), channel_id=1, source_target_pairs={{0,2},{1,3},{2,0},{3,1},{4,6},{5,7},{6,4},{7,5},{8,10},{9,11},{10,... | collective-permute-start | bytes 98312 | tf_op jit(solution)/shard_map/ppermute | solution.py:418
  54.9 5.1 %collective-permute-done.9.dense_one = bf16[32,512]{1,0:T(8,128)(2,1)S(1)} collective-permute-done((bf16[32,512]{1,0:T(8,128)(2,1)S(1)}, bf16[32,512]{1,0:T(8,128)(2,1)S(1)}, u32[]{:S(2)}, u32[]{:S(2)}) %collective-permute-start.9) | collective-permute-done | bytes 32800 | tf_op jit(solution)/shard_map/ppermute | solution.py:418
  59.9 2.8 %collective-permute-done.11.dense_three = bf16[32,512]{1,0:T(8,128)(2,1)S(1)} collective-permute-done((bf16[32,512]{1,0:T(8,128)(2,1)S(1)}, bf16[32,512]{1,0:T(8,128)(2,1)S(1)}, u32[]{:S(2)}, u32[]{:S(2)}) %collective-permute-start.11) | collective-permute-done | bytes 32800 | tf_op jit(solution)/shard_map/ppermute | solution.py:418
  62.7 0.1 gather.1
  62.8 16.9 %all_to_all.11.returned = bf16[64,2,512]{2,1,0:T(2,128)(2,1)S(1)} all-to-all(bf16[64,2,512]{2,1,0:T(2,128)(2,1)S(1)} %get-tuple-element.56), channel_id=1, replica_groups=mesh['ep'=64,'tp'=4] {'ep'}, dimensions={0} | all-to-all | bytes 262144 | tf_op jit(solution)/shard_map/all_to_all | solution.py:480
  79.7 0.8 combine.1
  (9 shorter events, 0.1 us)
Async XLA Ops:
  5.3 7.8 %collective-permute-start.2 = (bf16[16,2048]{1,0:T(8,128)(2,1)S(1)}, bf16[16,2048]{1,0:T(8,128)(2,1)S(1)}, u32[]{:S(2)}, u32[]{:S(2)}) collective-permute-start(bf16[16,2048]{1,0:T(8,128)(2,1)S(1)} %attend.1.after.own), channel_id=1, source_target_pairs={{0,3},{1,0},{2,1},{3,2},{4,7},{5,4},{6,5},{7,6},{8,11},{9,8},{10,9... | collective-permute-start | bytes 196616 | tf_op jit(solution)/shard_map/ppermute | solution.py:418
  8.6 4.7 %collective-permute-start.1 = (bf16[16,2048]{1,0:T(8,128)(2,1)S(1)}, bf16[16,2048]{1,0:T(8,128)(2,1)S(1)}, u32[]{:S(2)}, u32[]{:S(2)}) collective-permute-start(bf16[16,2048]{1,0:T(8,128)(2,1)S(1)} %attend.1.after.own), channel_id=1, source_target_pairs={{0,2},{1,3},{2,0},{3,1},{4,6},{5,7},{6,4},{7,5},{8,10},{9,11},{10,... | collective-permute-start | bytes 196616 | tf_op jit(solution)/shard_map/ppermute | solution.py:418
  9.2 4.8 %collective-permute-start = (bf16[16,2048]{1,0:T(8,128)(2,1)S(1)}, bf16[16,2048]{1,0:T(8,128)(2,1)S(1)}, u32[]{:S(2)}, u32[]{:S(2)}) collective-permute-start(bf16[16,2048]{1,0:T(8,128)(2,1)S(1)} %attend.1.after.own), channel_id=1, source_target_pairs={{0,1},{1,2},{2,3},{3,0},{4,5},{5,6},{6,7},{7,4},{8,9},{9,10},{10,1... | collective-permute-start | bytes 196616 | tf_op jit(solution)/shard_map/ppermute | solution.py:418
  38.9 4.7 %collective-permute-start.5 = (bf16[64,2,512]{2,1,0:T(2,128)(2,1)S(1)}, bf16[64,2,512]{2,1,0:T(2,128)(2,1)S(1)}, u32[]{:S(2)}, u32[]{:S(2)}) collective-permute-start(bf16[64,2,512]{2,1,0:T(2,128)(2,1)S(1)} %all_to_all.10.own), channel_id=1, source_target_pairs={{0,3},{1,0},{2,1},{3,2},{4,7},{5,4},{6,5},{7,6},{8,11},{9,8},{10,9... | collective-permute-start | bytes 393224 | tf_op jit(solution)/shard_map/ppermute | solution.py:418
  39.5 5.9 %collective-permute-start.4 = (bf16[64,2,512]{2,1,0:T(2,128)(2,1)S(1)}, bf16[64,2,512]{2,1,0:T(2,128)(2,1)S(1)}, u32[]{:S(2)}, u32[]{:S(2)}) collective-permute-start(bf16[64,2,512]{2,1,0:T(2,128)(2,1)S(1)} %all_to_all.10.own), channel_id=1, source_target_pairs={{0,2},{1,3},{2,0},{3,1},{4,6},{5,7},{6,4},{7,5},{8,10},{9,11},{10,... | collective-permute-start | bytes 393224 | tf_op jit(solution)/shard_map/ppermute | solution.py:418
  40.8 8.2 %collective-permute-start.3 = (bf16[64,2,512]{2,1,0:T(2,128)(2,1)S(1)}, bf16[64,2,512]{2,1,0:T(2,128)(2,1)S(1)}, u32[]{:S(2)}, u32[]{:S(2)}) collective-permute-start(bf16[64,2,512]{2,1,0:T(2,128)(2,1)S(1)} %all_to_all.10.own), channel_id=1, source_target_pairs={{0,1},{1,2},{2,3},{3,0},{4,5},{5,6},{6,7},{7,4},{8,9},{9,10},{10,1... | collective-permute-start | bytes 393224 | tf_op jit(solution)/shard_map/ppermute | solution.py:418
  49.7 13.0 %collective-permute-start.6 = (bf16[128,512]{1,0:T(8,128)(2,1)S(1)}, bf16[128,512]{1,0:T(8,128)(2,1)S(1)}, u32[]{:S(2)}, u32[]{:S(2)}) collective-permute-start(bf16[128,512]{1,0:T(8,128)(2,1)S(1)} %get-tuple-element.46), channel_id=1, source_target_pairs={{0,1},{1,2},{2,3},{3,0},{4,5},{5,6},{6,7},{7,4},{8,9},{9,10},{10,1... | collective-permute-start | bytes 393224 | tf_op jit(solution)/shard_map/ppermute | solution.py:418
  49.8 12.9 %collective-permute-start.7 = (bf16[128,512]{1,0:T(8,128)(2,1)S(1)}, bf16[128,512]{1,0:T(8,128)(2,1)S(1)}, u32[]{:S(2)}, u32[]{:S(2)}) collective-permute-start(bf16[128,512]{1,0:T(8,128)(2,1)S(1)} %get-tuple-element.47), channel_id=1, source_target_pairs={{0,2},{1,3},{2,0},{3,1},{4,6},{5,7},{6,4},{7,5},{8,10},{9,11},{10,... | collective-permute-start | bytes 393224 | tf_op jit(solution)/shard_map/ppermute | solution.py:418
  51.4 11.3 %collective-permute-start.8 = (bf16[128,512]{1,0:T(8,128)(2,1)S(1)}, bf16[128,512]{1,0:T(8,128)(2,1)S(1)}, u32[]{:S(2)}, u32[]{:S(2)}) collective-permute-start(bf16[128,512]{1,0:T(8,128)(2,1)S(1)} %get-tuple-element.48), channel_id=1, source_target_pairs={{0,3},{1,0},{2,1},{3,2},{4,7},{5,4},{6,5},{7,6},{8,11},{9,8},{10,9... | collective-permute-start | bytes 393224 | tf_op jit(solution)/shard_map/ppermute | solution.py:418
  53.4 6.5 %collective-permute-start.9 = (bf16[32,512]{1,0:T(8,128)(2,1)S(1)}, bf16[32,512]{1,0:T(8,128)(2,1)S(1)}, u32[]{:S(2)}, u32[]{:S(2)}) collective-permute-start(bf16[32,512]{1,0:T(8,128)(2,1)S(1)} %get-tuple-element.50), channel_id=1, source_target_pairs={{0,1},{1,2},{2,3},{3,0},{4,5},{5,6},{6,7},{7,4},{8,9},{9,10},{10,1... | collective-permute-start | bytes 98312 | tf_op jit(solution)/shard_map/ppermute | solution.py:418
  53.4 6.6 %collective-permute-start.10 = (bf16[32,512]{1,0:T(8,128)(2,1)S(1)}, bf16[32,512]{1,0:T(8,128)(2,1)S(1)}, u32[]{:S(2)}, u32[]{:S(2)}) collective-permute-start(bf16[32,512]{1,0:T(8,128)(2,1)S(1)} %get-tuple-element.51), channel_id=1, source_target_pairs={{0,2},{1,3},{2,0},{3,1},{4,6},{5,7},{6,4},{7,5},{8,10},{9,11},{10,... | collective-permute-start | bytes 98312 | tf_op jit(solution)/shard_map/ppermute | solution.py:418
  59.9 2.8 %collective-permute-start.11 = (bf16[32,512]{1,0:T(8,128)(2,1)S(1)}, bf16[32,512]{1,0:T(8,128)(2,1)S(1)}, u32[]{:S(2)}, u32[]{:S(2)}) collective-permute-start(bf16[32,512]{1,0:T(8,128)(2,1)S(1)} %get-tuple-element.52), channel_id=1, source_target_pairs={{0,3},{1,0},{2,1},{3,2},{4,7},{5,4},{6,5},{7,6},{8,11},{9,8},{10,9... | collective-permute-start | bytes 98312 | tf_op jit(solution)/shard_map/ppermute | solution.py:418
